TPU v7x, 512 devices: a whole 4x4x16 slice. The times are simulated.
512 devices in a mesh: sp: 32 (over z, core), tp: 16 (over y, x).
Axes of the slice: x: 4, y: 4, z: 16, core: 2. Of those that a mesh axis runs over, the one named last changes fastest.
Arguments:
- residual_in: bfloat16 [8192, 2048], P('sp'), may hold values from -3 to 3
- mix_gain: float32 [2048], replicated, may hold values from 0.1 to 1.9
- pool_weight: bfloat16 [512, 2048], P(None, 'tp'), may hold values from -0.5 to 0.5
- pool_scale: float32 [2048], P('tp'), may hold values from 0.1 to 1.9
- ffn_gain: float32 [2048], replicated, may hold values from 0.1 to 1.9
- route_ids: int32 [8192, 2], P('sp'), may hold values from 0 to 31, all different within a row; in each aligned block of 16 rows (0 to 15, 16 to 31, ...) at most 2 rows name the same one
- route_weights: float32 [8192, 2], P('sp'), may hold values from 0.1 to 1
- gate_weight: bfloat16 [32, 2048, 3584], P('sp', None, 'tp'), may hold values from -0.125 to 0.125
- up_weight: bfloat16 [32, 2048, 3584], P('sp', None, 'tp'), may hold values from -0.125 to 0.125
- down_weight: bfloat16 [32, 3584, 2048], P('sp', 'tp'), may hold values from -0.09375 to 0.09375
Outputs:
- layer_out: bfloat16 [8192, 2048], P('sp')
Inputs may be any that keep to these rules, and one draw needn't show every extreme that they name: `route_ids`: each row names 2 different experts; in each aligned block of 16 rows no expert is named by more than 2 rows, and some block has an expert named by exactly 2 rows.
All inputs are finite; a program needn't handle non-finite values.
Results may differ from a plain program's by a relative error of at most 0.0074.
Values may be sent and summed in bfloat16 or wider, within the bound.
No kernel may reach another device: no remote copies, remote signals or barrier semaphores. Data moves between devices by JAX's collectives and lax.ppermute only.
A program may use at most 64 MiB of HBM per device.

v0:
```python
import jax
import jax.numpy as jnp
from jax import lax
from jax.sharding import Mesh
from jax.sharding import PartitionSpec as P

GROUPS = 4
SPAN = 16
TOP_K = 2
SP = ("sp_0", "sp_1")


EPS = 1e-06


def from_behind(value, axis, steps):
    count = lax.axis_size(axis)
    first, last = (max(0, -steps), min(count, count - steps))
    return lax.ppermute(value, axis, [(source, source + steps) for source in range(first, last)])


def split_up(shard, dim, size):
    before, after = (shard.shape[:dim], shard.shape[dim + 1 :])
    return jnp.moveaxis(shard.reshape(*before, size, -1, *after), dim, 0)


def sent_and_summed(shard, axis, dim):
    size = lax.axis_size(axis)
    blocks = lax.all_to_all(split_up(shard, dim, size), axis, 0, 0, tiled=True)
    return jnp.sum(blocks.astype(jnp.float32), axis=0)


def in_order(blocks, dim):
    dims = list(blocks.shape[1:])
    dims[dim] *= blocks.shape[0]
    return jnp.moveaxis(blocks, 0, dim).reshape(dims)


def exchange_in_order(blocks, axes, order):
    dims = [lax.axis_size(a) for a in axes]
    blocks = blocks.reshape(*dims, *blocks.shape[1:])
    for k in order:
        blocks = lax.all_to_all(blocks, axes[k], split_axis=k, concat_axis=k, tiled=True)
    return blocks.reshape(-1, *blocks.shape[len(axes) :])


def core_and_chips(shard, groups, order, split_dim, concat_dim):
    size = lax.axis_size(groups[0]) * lax.axis_size(groups[1])
    blocks = split_up(shard, split_dim, size)
    return in_order(exchange_in_order(blocks, groups, order), concat_dim)


def copy_for_each(shard, axis):
    size = lax.axis_size(axis)
    return lax.all_to_all(
        jnp.broadcast_to(shard[None], (size, *shard.shape)), axis, 0, 0, tiled=True
    )


def gather_directly(shard, axis, dim):
    blocks = copy_for_each(shard, axis)
    return in_order(blocks, dim)


def rms_scale(values, gain):
    return values * lax.rsqrt(jnp.mean(values * values, axis=-1, keepdims=True) + EPS) * gain


def slot_table(chosen_ids, experts, capacity):
    flat_ids = chosen_ids.reshape(-1)
    matches = (flat_ids[:, None] == jnp.arange(experts, dtype=jnp.int32)[None, :]).astype(jnp.int32)
    before = jnp.cumsum(matches, axis=0) - matches
    slot_of = jnp.sum(before * matches, axis=1)
    target = flat_ids * capacity + slot_of
    return (target[:, None] == jnp.arange(experts * capacity, dtype=jnp.int32)[None, :]).astype(
        jnp.float32
    )


def shards(
    residual_in,
    mix_gain,
    pool_weight,
    pool_scale,
    ffn_gain,
    route_ids,
    route_weights,
    gate_weight,
    up_weight,
    down_weight,
):
    tp_count = lax.axis_size("tp")
    sp_count = lax.axis_size(SP)
    tp_index = lax.axis_index("tp")
    tok_count, width = residual_in.shape
    group_width = width // GROUPS
    col_count = pool_weight.shape[1]
    row_count = tok_count // tp_count
    capacity = 2 * TOP_K * row_count // sp_count
    group_index = tp_index * col_count // group_width
    window = jnp.power(2, group_index + 1)
    stream = residual_in.astype(jnp.float32)
    inverse = lax.rsqrt(jnp.mean(stream * stream, axis=-1, keepdims=True) + EPS)
    stream_group = lax.dynamic_slice_in_dim(stream, group_index * group_width, group_width, 1)
    gain_group = lax.dynamic_slice_in_dim(mix_gain, group_index * group_width, group_width, 0)
    normed_group = (stream_group * inverse * gain_group).astype(jnp.bfloat16)
    rim_rows = from_behind(normed_group[tok_count - SPAN :], SP, 1)
    extended = jnp.concatenate([rim_rows, normed_group], axis=0).astype(jnp.float32)
    window_sum = jnp.zeros((tok_count, group_width), jnp.float32)
    for offset in range(SPAN):
        window_sum = window_sum + jnp.where(
            offset < window, extended[SPAN - offset : SPAN - offset + tok_count], 0.0
        )
    position = lax.axis_index(SP) * tok_count + jnp.arange(tok_count, dtype=jnp.int32)
    divisor = jnp.minimum(position + 1, window).astype(jnp.float32)
    pooled = (window_sum / divisor[:, None] - extended[SPAN:]).astype(jnp.bfloat16)
    mixed = (jnp.dot(pooled, pool_weight, preferred_element_type=jnp.float32) * pool_scale).astype(
        jnp.bfloat16
    )
    stream_own = lax.dynamic_slice_in_dim(stream, tp_index * row_count, row_count, 0)
    mixed_own = lax.all_to_all(mixed, "tp", split_axis=0, concat_axis=1, tiled=True)
    after_own = (stream_own + mixed_own.astype(jnp.float32)).astype(jnp.bfloat16)
    normed_own = rms_scale(after_own.astype(jnp.float32), ffn_gain).astype(jnp.bfloat16)
    ids_own = lax.dynamic_slice_in_dim(route_ids, tp_index * row_count, row_count, 0)
    table_own = slot_table(ids_own, sp_count, capacity)
    repeated = jnp.repeat(normed_own, TOP_K, axis=0)
    outgoing = lax.dot_general(
        table_own.astype(jnp.bfloat16),
        repeated,
        (((0,), (0,)), ((), ())),
        preferred_element_type=jnp.float32,
    )
    outgoing = outgoing.astype(jnp.bfloat16).reshape(sp_count, capacity, width)
    arrived = lax.all_to_all(outgoing, SP, split_axis=0, concat_axis=0, tiled=True)
    piece = lax.all_gather(arrived, "tp", axis=0, tiled=True)
    flat_rows = piece.reshape(-1, width)
    gate_part = jnp.dot(flat_rows, gate_weight[0], preferred_element_type=jnp.float32)
    up_part = jnp.dot(flat_rows, up_weight[0], preferred_element_type=jnp.float32)
    hidden = (jax.nn.silu(gate_part) * up_part).astype(jnp.bfloat16)
    hidden_all = hidden.reshape(piece.shape[0], piece.shape[1], hidden.shape[1])
    hidden_flat = hidden_all.reshape(-1, hidden_all.shape[-1])
    term = jnp.dot(hidden_flat, down_weight[0], preferred_element_type=jnp.float32)
    summed = sent_and_summed(
        term.astype(jnp.bfloat16).astype(jnp.float32).astype(jnp.bfloat16), "tp", 0
    )
    expert_out = summed.astype(jnp.bfloat16).reshape(sp_count, capacity, width)
    returned_rows = core_and_chips(expert_out, ("sp_0", "sp_1"), (1, 0), 0, 0)
    weights_own = lax.dynamic_slice_in_dim(route_weights, tp_index * row_count, row_count, 0)
    weight_table = jnp.einsum(
        "rk,rkc->rc", weights_own, table_own.reshape(row_count, TOP_K, sp_count * capacity)
    )
    expert_mix = jnp.dot(
        weight_table,
        returned_rows.reshape(-1, width).astype(jnp.float32),
        precision=lax.Precision.HIGHEST,
    )
    out_own = (after_own.astype(jnp.float32) + expert_mix).astype(jnp.bfloat16)
    return gather_directly(out_own, "tp", 0)


def solution(mesh):
    torus = Mesh(mesh.devices.reshape(16, 2, mesh.shape["tp"]), ("sp_0", "sp_1", "tp"))
    return jax.shard_map(
        shards,
        mesh=torus,
        in_specs=(
            P(SP, None),
            P(),
            P(None, "tp"),
            P("tp"),
            P(),
            P(SP, None),
            P(SP, None),
            P(SP, None, "tp"),
            P(SP, None, "tp"),
            P(SP, "tp", None),
        ),
        out_specs=P(SP, None),
        check_vma=False,
    )
```

profile of v0, /device:TPU:32, one launch (start us, length us, event | category | flops | bytes accessed | tf_op | source)
XLA Modules:
  0.0 268.7 jit_solution(1426922073096499499)
XLA Ops:
  6.5 1.6 multiply_reduce_fusion
  8.1 1.5 convert_element_type.67
  9.6 0.8 dynamic_slice.17
  10.4 0.1 multiply_convert_fusion
  10.5 1.9 collective-permute-start
  12.5 0.1 constant_dynamic-slice_fusion
  12.6 0.1 copy.24
  12.7 0.1 eq.35
  12.8 0.1 fusion.40
  12.8 0.1 reduce_window_sum.11
  12.9 0.2 select_reduce_fusion
  13.1 2.5 collective-permute-done
  15.6 0.1 maximum_convert_fusion
  15.7 0.0 copy-start.1
  15.7 2.0 fusion.2
  17.7 7.0 %all-to-all-start = ((bf16[16,16,128]{2,1,0:T(8,128)(2,1)}), bf16[16,16,128]{2,1,0:T(8,128)(2,1)S(1)}, u32[]{:S(2)}, u32[]{:S(2)}) async-start(bf16[16,16,128]{2,1,0:T(8,128)(2,1)} %bitcast), calls=%async_computation | async-start | bytes 131072 | tf_op jit(solution)/shard_map/all_to_all | solution.py:121
  24.8 0.0 all-gather.2.cloned.1.call-start
  24.8 7.6 %all-to-all-done = bf16[16,16,128]{2,1,0:T(8,128)(2,1)S(1)} async-done(((bf16[16,16,128]{2,1,0:T(8,128)(2,1)}), bf16[16,16,128]{2,1,0:T(8,128)(2,1)S(1)}, u32[]{:S(2)}, u32[]{:S(2)}) %all-to-all-start) | async-done | bytes 65568 | tf_op jit(solution)/shard_map/all_to_all | solution.py:121
  32.4 0.1 fusion.33
  32.6 0.1 fusion.35
  32.7 0.1 broadcast_in_dim.38
  32.8 0.1 reshape.67
  32.8 0.3 convolution_convert_fusion.1
  33.2 0.2 reshape.68
  33.3 37.4 %all_to_all.38 = bf16[32,2,2048]{2,1,0:T(2,128)(2,1)} all-to-all(bf16[32,2,2048]{2,1,0:T(2,128)(2,1)S(1)} %reshape.68), channel_id=1, replica_groups=mesh['sp_0'=16,'sp_1'=2,'tp'=16] {'sp_0','sp_1'}, dimensions={0} | all-to-all | bytes 524288 | tf_op jit(solution)/shard_map/all_to_all | solution.py:134
  70.8 0.0 all-gather.2.cloned.1.call-update
  70.8 0.0 copy-start.3
  70.8 56.0 %all-gather.2.cloned.1.call-done = bf16[512,2,2048]{2,1,0:T(2,128)(2,1)} async-done(((bf16[32,2,2048]{2,1,0:T(2,128)(2,1)}), bf16[512,2,2048]{2,1,0:T(2,128)(2,1)}) %all-gather.2.cloned.1.call-update) | async-done | bytes 4194320 | tf_op jit(solution)/shard_map/all_gather | solution.py:135
  126.8 7.2 %reshape.69 = bf16[1024,2048]{1,0:T(8,128)(2,1)} reshape(bf16[512,2,2048]{2,1,0:T(2,128)(2,1)} %all-gather.2.cloned.1.call-done) | data formatting | bytes 8388608 | tf_op jit(solution)/shard_map/reshape | solution.py:136
  134.0 4.6 %fusion.6 = f32[1024,224]{0,1:T(8,128)} fusion(bf16[1024,2048]{1,0:T(8,128)(2,1)} %reshape.69, bf16[1,2048,224]{1,2,0:T(8,128)(2,1)S(1)} %copy-done.3), kind=kOutput, calls=%fused_computation.11 | convolution fusion | flops 939524096 | bytes 6029312 | tf_op jit(solution)/shard_map/dot_general | solution.py:137
  138.6 7.0 %convolution_convert_fusion = bf16[1024,2048]{1,0:T(8,128)(2,1)} fusion(bf16[1024,2048]{1,0:T(8,128)(2,1)} %reshape.69, bf16[1,224,2048]{2,1,0:T(8,128)(2,1)S(1)} %copy-done, bf16[1,2048,224]{1,2,0:T(8,128)(2,1)S(1)} %copy-done.4, f32[1024,224]{0,1:T(8,128)} %fusion.6), kind=kOutput, calls=%fused_computation | convolution fusion | flops 1882521600 | bytes 11141120 | tf_op jit(solution)/shard_map/dot_general | solution.py:142
  145.6 56.0 %all_to_all.39 = bf16[16,64,2048]{2,1,0:T(8,128)(2,1)} all-to-all(bf16[16,64,2048]{2,1,0:T(8,128)(2,1)} %bitcast.35), channel_id=1, replica_groups=mesh['sp_0'=16,'sp_1'=2,'tp'=16] {'tp'}, dimensions={0} | all-to-all | bytes 8388608 | tf_op jit(solution)/shard_map/all_to_all | solution.py:29
  201.7 3.0 %reduce_sum.45 = bf16[64,2048]{1,0:T(8,128)(2,1)S(1)} reduce(bf16[16,64,2048]{2,1,0:T(8,128)(2,1)} %all_to_all.39, bf16[]{:T(256)} %constant.97.clone.1), dimensions={0}, to_apply=%region_4.5 | reduce | flops 1966080 | bytes 4456450 | tf_op jit(solution)/shard_map/reduce_sum | solution.py:30
  204.6 0.2 reshape_reshape_reshape.6
  204.8 0.2 copy.20
  205.0 3.9 %all_to_all.40 = bf16[16,2,1,2,2048]{4,3,0,2,1:T(2,128)(2,1)S(1)} all-to-all(bf16[16,2,1,2,2048]{4,3,0,2,1:T(2,128)(2,1)S(1)} %copy.20), channel_id=1, replica_groups=mesh['sp_0'=16,'sp_1'=2,'tp'=16] {'sp_1'}, dimensions={1} | all-to-all | bytes 524288 | tf_op jit(solution)/shard_map/all_to_all | solution.py:43
  209.0 1.0 copy.21
  209.9 12.7 %all-to-all-start.4 = ((bf16[16,2,1,2,2048]{4,3,1,2,0:T(2,128)(2,1)}), bf16[16,2,1,2,2048]{4,3,1,2,0:T(2,128)(2,1)S(1)}, u32[]{:S(2)}, u32[]{:S(2)}) async-start(bf16[16,2,1,2,2048]{4,3,1,2,0:T(2,128)(2,1)} %copy.21), calls=%async_computation.4 | async-start | bytes 524288 | tf_op jit(solution)/shard_map/all_to_all | solution.py:43
  222.6 0.1 reduce_sum.43
  222.7 0.8 dynamic-slice_bitcast_fusion
  223.4 0.1 copy.22
  223.5 0.2 fusion.37
  223.7 17.2 %all-to-all-done.4 = bf16[16,2,1,2,2048]{4,3,1,2,0:T(2,128)(2,1)S(1)} async-done(((bf16[16,2,1,2,2048]{4,3,1,2,0:T(2,128)(2,1)}), bf16[16,2,1,2,2048]{4,3,1,2,0:T(2,128)(2,1)S(1)}, u32[]{:S(2)}, u32[]{:S(2)}) %all-to-all-start.4) | async-done | bytes 262176 | tf_op jit(solution)/shard_map/all_to_all | solution.py:43
  241.0 0.1 reshape_reshape_reshape.7
  241.1 0.2 fusion
  241.3 0.1 broadcast_in_dim.39
  241.4 19.5 %all_to_all.41 = bf16[16,16,2048]{2,1,0:T(8,128)(2,1)S(1)} all-to-all(bf16[16,16,2048]{2,1,0:T(8,128)(2,1)S(1)} %broadcast_in_dim.39), channel_id=1, replica_groups=mesh['sp_0'=16,'sp_1'=2,'tp'=16] {'tp'}, dimensions={0} | all-to-all | bytes 2097152 | tf_op jit(solution)/shard_map/all_to_all | solution.py:55
  260.9 1.0 copy.29
  (18 shorter events, 0.1 us)
Async XLA Ops:
  6.5 132.1 %copy-start = (bf16[1,224,2048]{2,1,0:T(8,128)(2,1)S(1)}, bf16[1,224,2048]{2,1,0:T(8,128)(2,1)}, u32[]{:S(2)}) copy-start(bf16[1,224,2048]{2,1,0:T(8,128)(2,1)} %param.19) | copy-start | bytes 2752516
  6.5 6.0 %copy-start.2 = (s32[256,2]{0,1:T(2,128)S(1)}, s32[256,2]{0,1:T(2,128)}, u32[]{:S(2)}) copy-start(s32[256,2]{0,1:T(2,128)} %param.15) | copy-start | bytes 6148
  6.5 9.1 %copy-start.6 = (f32[128]{0:T(128)S(1)}, f32[128]{0:T(128)}, u32[]{:S(2)}) copy-start(f32[128]{0:T(128)} %param.13) | copy-start | bytes 1540
  6.5 9.1 %copy-start.5 = (bf16[512,128]{1,0:T(8,128)(2,1)S(1)}, bf16[512,128]{1,0:T(8,128)(2,1)}, u32[]{:S(2)}) copy-start(bf16[512,128]{1,0:T(8,128)(2,1)} %param.12) | copy-start | bytes 393220
  10.5 5.1 %collective-permute-start = (bf16[16,512]{1,0:T(8,128)(2,1)S(1)}, bf16[16,512]{1,0:T(8,128)(2,1)S(1)}, u32[]{:S(2)}, u32[]{:S(2)}) collective-permute-start(bf16[16,512]{1,0:T(8,128)(2,1)S(1)} %slice.69), channel_id=1, source_target_pairs={{0,16},{16,32},{32,48},{48,64},{64,80},{80,96},{96,112},{112,128},... | collective-permute-start | bytes 49160 | tf_op jit(solution)/shard_map/ppermute | solution.py:19
  15.7 16.9 %copy-start.1 = (f32[2048]{0:T(1024)S(1)}, f32[2048]{0:T(1024)}, u32[]{:S(2)}) copy-start(f32[2048]{0:T(1024)} %param.14) | copy-start | bytes 24580
  17.7 14.7 %all-to-all-start = ((bf16[16,16,128]{2,1,0:T(8,128)(2,1)}), bf16[16,16,128]{2,1,0:T(8,128)(2,1)S(1)}, u32[]{:S(2)}, u32[]{:S(2)}) async-start(bf16[16,16,128]{2,1,0:T(8,128)(2,1)} %bitcast), calls=%async_computation | async-start | bytes 131072 | tf_op jit(solution)/shard_map/all_to_all | solution.py:121
  24.8 102.0 %all-gather.2.cloned.1.call-start = ((), (), s32[]{:S(2)}) async-start(), calls=%async_computation.6 | async-start | bytes 4456448 | tf_op jit(solution)/shard_map/all_gather | solution.py:135
  70.8 63.2 %copy-start.3 = (bf16[1,2048,224]{1,2,0:T(8,128)(2,1)S(1)}, bf16[1,2048,224]{1,2,0:T(8,128)(2,1)}, u32[]{:S(2)}) copy-start(bf16[1,2048,224]{1,2,0:T(8,128)(2,1)} %param.17) | copy-start | bytes 2752516
  134.0 4.6 %copy-start.4 = (bf16[1,2048,224]{1,2,0:T(8,128)(2,1)S(1)}, bf16[1,2048,224]{1,2,0:T(8,128)(2,1)}, u32[]{:S(2)}) copy-start(bf16[1,2048,224]{1,2,0:T(8,128)(2,1)} %param.18) | copy-start | bytes 2752516
  209.9 31.0 %all-to-all-start.4 = ((bf16[16,2,1,2,2048]{4,3,1,2,0:T(2,128)(2,1)}), bf16[16,2,1,2,2048]{4,3,1,2,0:T(2,128)(2,1)S(1)}, u32[]{:S(2)}, u32[]{:S(2)}) async-start(bf16[16,2,1,2,2048]{4,3,1,2,0:T(2,128)(2,1)} %copy.21), calls=%async_computation.4 | async-start | bytes 524288 | tf_op jit(solution)/shard_map/all_to_all | solution.py:43
Sparse Core Ops, SparseCore 0:
  70.9 55.8 all-gather.1
where the time goes:
time: 269 us
  blocking collectives  117 us (43%)
  waiting for transfers between devices  83.3 us (31%)
  starting transfers between devices  21.7 us (8%)
  matrix products  14.4 us (5%)
  between operations  13.7 us (5%)
  local copies, waits for them, and re-layouts  12 us (4%)
  other arithmetic  6.75 us (3%)
    all_to_all x1, blocking collectives, sent_and_summed(): blocks = lax.all_to_all(split_up(shard, dim, size), axis, 0, 0, tiled=True)  56 us
    all_gather x1, waiting for transfers between devices, shards(): piece = lax.all_gather(arrived, 'tp', axis=0, tiled=True)  56 us
    all_to_all x1, blocking collectives, shards(): lax.all_to_all(outgoing, SP, split_axis=0, concat_axis=0, tiled=True)  37.4 us
    all_to_all x1, blocking collectives, copy_for_each(): lax.all_to_all(jnp.broadcast_to(shard[None], (size, *shard.shape)), axis,...  19.5 us
    all_to_all x1, waiting for transfers between devices, exchange_in_order(): lax.all_to_all(blocks, axes[k], split_axis=k, concat_axis=k, tiled=True)  17.2 us
    all_to_all x1, starting transfers between devices, exchange_in_order(): lax.all_to_all(blocks, axes[k], split_axis=k, concat_axis=k, tiled=True)  12.7 us
    all_to_all x1, waiting for transfers between devices, shards(): lax.all_to_all(mixed, 'tp', split_axis=0, concat_axis=1, tiled=True)  7.6 us
    reshape x1, local copies, waits for them, and re-layouts, shards(): flat_rows = piece.reshape(-1, width)  7.21 us
  transfers between devices with their start and end apart: 4, of which 4 were waited for; matrix products, arithmetic and copies ran while one was open for 1% of the time, Pallas kernels for 0%

commit v1 on v0

v1 whole, which is shorter than its diff:
```python
import math

import jax
import jax.numpy as jnp
import numpy as np
from jax import lax
from jax.sharding import Mesh
from jax.sharding import PartitionSpec as P

GROUPS = 4
SPAN = 16
TOP_K = 2
SP = ("z", "c")
TP = ("y", "x")
ALL = ("z", "c", "y", "x")


EPS = 1e-06


def from_behind(value, axis, steps):
    count = lax.axis_size(axis)
    first, last = (max(0, -steps), min(count, count - steps))
    return lax.ppermute(value, axis, [(source, source + steps) for source in range(first, last)])


def rms_scale(values, gain):
    return values * lax.rsqrt(jnp.mean(values * values, axis=-1, keepdims=True) + EPS) * gain


def plane_groups(swapped):
    sizes = [lax.axis_size(a) for a in ALL]
    index = np.arange(math.prod(sizes)).reshape(sizes)
    groups = []
    for z in range(sizes[0]):
        for c in range(sizes[1]):
            plane = index[z, c]
            groups += (plane if (c % 2 == 0) != swapped else plane.T).tolist()
    return groups


def exchange(blocks, groups):
    return lax.all_to_all(blocks, ALL, 0, 0, tiled=True, axis_index_groups=groups)


def gather_stage(rows, groups):
    blocks = jnp.broadcast_to(rows[None], (len(groups[0]), *rows.shape))
    return exchange(blocks, groups).reshape(-1, rows.shape[-1])


def sum_stage(rows, groups):
    blocks = exchange(rows.reshape(len(groups[0]), -1, rows.shape[-1]), groups)
    return jnp.sum(blocks.astype(jnp.float32), axis=0).astype(jnp.bfloat16)


def slot_table(chosen_ids, experts, capacity):
    flat_ids = chosen_ids.reshape(-1)
    matches = (flat_ids[:, None] == jnp.arange(experts, dtype=jnp.int32)[None, :]).astype(jnp.int32)
    before = jnp.cumsum(matches, axis=0) - matches
    slot_of = jnp.sum(before * matches, axis=1)
    target = flat_ids * capacity + slot_of
    table = target[:, None] == jnp.arange(experts * capacity, dtype=jnp.int32)[None, :]
    return table.astype(jnp.float32).reshape(*chosen_ids.shape, experts * capacity)


def shards(
    residual_in,
    mix_gain,
    pool_weight,
    pool_scale,
    ffn_gain,
    route_ids,
    route_weights,
    gate_weight,
    up_weight,
    down_weight,
):
    tp_count = lax.axis_size(TP)
    sp_count = lax.axis_size(SP)
    tp_index = lax.axis_index(TP)
    tok_count, width = residual_in.shape
    group_width = width // GROUPS
    col_count = pool_weight.shape[1]
    row_count = tok_count // tp_count
    capacity = 2 * TOP_K * row_count // sp_count
    group_index = tp_index * col_count // group_width
    window = jnp.power(2, group_index + 1)
    stream = residual_in.astype(jnp.float32)
    inverse = lax.rsqrt(jnp.mean(stream * stream, axis=-1, keepdims=True) + EPS)
    stream_group = lax.dynamic_slice_in_dim(stream, group_index * group_width, group_width, 1)
    gain_group = lax.dynamic_slice_in_dim(mix_gain, group_index * group_width, group_width, 0)
    normed_group = (stream_group * inverse * gain_group).astype(jnp.bfloat16)
    rim_rows = from_behind(normed_group[tok_count - SPAN :], SP, 1)
    extended = jnp.concatenate([rim_rows, normed_group], axis=0).astype(jnp.float32)
    window_sum = jnp.zeros((tok_count, group_width), jnp.float32)
    for offset in range(SPAN):
        window_sum = window_sum + jnp.where(
            offset < window, extended[SPAN - offset : SPAN - offset + tok_count], 0.0
        )
    position = lax.axis_index(SP) * tok_count + jnp.arange(tok_count, dtype=jnp.int32)
    divisor = jnp.minimum(position + 1, window).astype(jnp.float32)
    pooled = (window_sum / divisor[:, None] - extended[SPAN:]).astype(jnp.bfloat16)
    mixed = (jnp.dot(pooled, pool_weight, preferred_element_type=jnp.float32) * pool_scale).astype(
        jnp.bfloat16
    )
    stream_own = lax.dynamic_slice_in_dim(stream, tp_index * row_count, row_count, 0)
    mixed_own = lax.all_to_all(mixed, TP, split_axis=0, concat_axis=1, tiled=True)
    after_own = (stream_own + mixed_own.astype(jnp.float32)).astype(jnp.bfloat16)
    normed_own = rms_scale(after_own.astype(jnp.float32), ffn_gain).astype(jnp.bfloat16)
    ids_own = lax.dynamic_slice_in_dim(route_ids, tp_index * row_count, row_count, 0)
    table_own = slot_table(ids_own, sp_count, capacity)
    outgoing = lax.dot_general(
        jnp.sum(table_own, axis=1).astype(jnp.bfloat16),
        normed_own,
        (((0,), (0,)), ((), ())),
        preferred_element_type=jnp.float32,
    )
    outgoing = outgoing.astype(jnp.bfloat16).reshape(sp_count, capacity, width)
    arrived = lax.all_to_all(outgoing, SP, split_axis=0, concat_axis=0, tiled=True)
    first, second = (plane_groups(False), plane_groups(True))
    flat_rows = gather_stage(gather_stage(arrived.reshape(-1, width), first), second)
    gate_part = jnp.dot(flat_rows, gate_weight[0], preferred_element_type=jnp.float32)
    up_part = jnp.dot(flat_rows, up_weight[0], preferred_element_type=jnp.float32)
    hidden = (jax.nn.silu(gate_part) * up_part).astype(jnp.bfloat16)
    term = jnp.dot(hidden, down_weight[0], preferred_element_type=jnp.float32).astype(jnp.bfloat16)
    expert_out = sum_stage(sum_stage(term, second), first)
    returned_rows = lax.all_to_all(
        expert_out.reshape(sp_count, capacity, width), SP, split_axis=0, concat_axis=0, tiled=True
    )
    weights_own = lax.dynamic_slice_in_dim(route_weights, tp_index * row_count, row_count, 0)
    weight_table = jnp.sum(weights_own[:, :, None] * table_own, axis=1)
    expert_mix = jnp.dot(
        weight_table,
        returned_rows.reshape(-1, width).astype(jnp.float32),
        precision=lax.Precision.HIGHEST,
    )
    out_own = (after_own.astype(jnp.float32) + expert_mix).astype(jnp.bfloat16)
    copies = jnp.broadcast_to(out_own[None], (tp_count, *out_own.shape))
    return lax.all_to_all(copies, TP, 0, 0, tiled=True).reshape(tok_count, width)


def solution(mesh):
    torus = Mesh(mesh.devices.reshape(-1, 2, 4, mesh.shape["tp"] // 4), ALL)
    return jax.shard_map(
        shards,
        mesh=torus,
        in_specs=(
            P(SP, None),
            P(),
            P(None, TP),
            P(TP),
            P(),
            P(SP, None),
            P(SP, None),
            P(SP, None, TP),
            P(SP, None, TP),
            P(SP, TP, None),
        ),
        out_specs=P(SP, None),
        check_vma=False,
    )
```

time: 269 us -> 217 us (0.81)
  the two profiles are of different devices: /device:TPU:32 before, /device:TPU:1 now
where the time goes in v1:
time: 217 us; the launch traced here: 216 us
  blocking collectives  174 us (80%)
  matrix products  10.7 us (5%)
  waiting for transfers between devices  9.62 us (4%)
  starting transfers between devices  8.77 us (4%)
  other arithmetic  7.05 us (3%)
  local copies, waits for them, and re-layouts  5.53 us (3%)
    all_to_all x4, blocking collectives, exchange(): lax.all_to_all(blocks, ALL, 0, 0, tiled=True, axis_index_groups=groups)  86.6 us
    all_to_all x1, blocking collectives, shards(): lax.all_to_all(outgoing, SP, split_axis=0, concat_axis=0, tiled=True)  40.3 us
    all_to_all x1, blocking collectives, shards(): lax.all_to_all(expert_out.reshape(sp_count, capacity, width), SP, split_a...  28.9 us
    all_to_all x1, blocking collectives, shards(): lax.all_to_all(copies, TP, 0, 0, tiled=True).reshape(tok_count, width)  18.4 us
    dot_general x1, matrix products, shards(): jnp.dot(hidden, down_weight[0], preferred_element_type=jnp.float32)  6.72 us
    all_to_all x1, waiting for transfers between devices, shards(): lax.all_to_all(mixed, TP, split_axis=0, concat_axis=1, tiled=True)  6.71 us
    ppermute x1, starting transfers between devices, from_behind(): lax.ppermute(value, axis, [(source, source + steps) for source in range(f...  4.92 us
  transfers between devices with their start and end apart: 2, of which 2 were waited for; matrix products, arithmetic and copies ran while one was open for 0% of the time, Pallas kernels for 0%

profile of v1, /device:TPU:1, one launch (start us, length us, event | category | flops | bytes accessed | tf_op | source)
XLA Modules:
  0.0 216.2 jit_solution(405147300941553626)
XLA Ops:
  0.0 1.6 multiply_reduce_fusion
  1.6 1.5 convert_element_type.68
  3.1 0.8 dynamic_slice.17
  3.9 0.1 multiply_convert_fusion
  4.0 4.9 %collective-permute-start = (bf16[16,512]{1,0:T(8,128)(2,1)S(1)}, bf16[16,512]{1,0:T(8,128)(2,1)S(1)}, u32[]{:S(2)}, u32[]{:S(2)}) collective-permute-start(bf16[16,512]{1,0:T(8,128)(2,1)S(1)} %slice.69), channel_id=1, source_target_pairs={{0,16},{16,32},{32,48},{48,64},{64,80},{80,96},{96,112},{112,128},... | collective-permute-start | bytes 49160 | tf_op jit(solution)/shard_map/ppermute | solution.py:24
  9.0 0.1 constant_dynamic-slice_fusion.1
  9.1 0.1 constant_dynamic-slice_fusion
  9.2 0.1 copy.20
  9.2 0.1 eq.29
  9.3 0.1 fusion.40
  9.4 0.1 reduce_window_sum.11
  9.5 0.2 select_reduce_fusion.1
  9.6 0.1 reduce_sum.73
  9.8 0.1 copy.19
  9.9 2.9 %collective-permute-done = bf16[16,512]{1,0:T(8,128)(2,1)S(1)} collective-permute-done((bf16[16,512]{1,0:T(8,128)(2,1)S(1)}, bf16[16,512]{1,0:T(8,128)(2,1)S(1)}, u32[]{:S(2)}, u32[]{:S(2)}) %collective-permute-start) | collective-permute-done | bytes 16416 | tf_op jit(solution)/shard_map/ppermute | solution.py:24
  12.8 0.1 maximum_convert_fusion
  12.9 0.0 copy-done.8
  12.9 0.0 copy-done.7
  12.9 0.0 copy-start.2
  12.9 2.0 fusion.2
  15.0 3.8 %all-to-all-start = ((bf16[16,16,128]{2,1,0:T(8,128)(2,1)}), bf16[16,16,128]{2,1,0:T(8,128)(2,1)S(1)}, u32[]{:S(2)}, u32[]{:S(2)}) async-start(bf16[16,16,128]{2,1,0:T(8,128)(2,1)} %bitcast), calls=%async_computation | async-start | bytes 131072 | tf_op jit(solution)/shard_map/all_to_all | solution.py:107
  18.8 0.1 convert_reduce_fusion
  18.9 6.7 %all-to-all-done = bf16[16,16,128]{2,1,0:T(8,128)(2,1)S(1)} async-done(((bf16[16,16,128]{2,1,0:T(8,128)(2,1)}), bf16[16,16,128]{2,1,0:T(8,128)(2,1)S(1)}, u32[]{:S(2)}, u32[]{:S(2)}) %all-to-all-start) | async-done | bytes 65568 | tf_op jit(solution)/shard_map/all_to_all | solution.py:107
  25.6 0.1 fusion.33
  25.7 0.0 copy-done.2
  25.7 0.3 convolution_convert_fusion.1
  26.0 0.2 reshape.75
  26.2 40.3 %all_to_all.48 = bf16[32,2,2048]{2,1,0:T(2,128)(2,1)S(1)} all-to-all(bf16[32,2,2048]{2,1,0:T(2,128)(2,1)S(1)} %reshape.75), channel_id=1, replica_groups=mesh['z'=16,'c'=2,'y'=4,'x'=4] {'z','c'}, dimensions={0} | all-to-all | bytes 524288 | tf_op jit(solution)/shard_map/all_to_all | solution.py:119
  66.6 0.1 broadcast_in_dim.50
  66.7 0.1 broadcast_in_dim.51
  66.8 12.2 %all_to_all.49 = bf16[4,64,2048]{2,1,0:T(8,128)(2,1)S(1)} all-to-all(bf16[4,64,2048]{2,1,0:T(8,128)(2,1)S(1)} %broadcast_in_dim.51), channel_id=1, replica_groups={{0,1,2,3},{4,5,6,7},{8,9,10,11},{12,13,14,15},{16,20,24,28},{17,21,25,2..., dimensions={0} | all-to-all | bytes 2097152 | tf_op jit(solution)/shard_map/all_to_all | solution.py:43
  79.0 0.5 broadcast_in_dim.53
  79.5 0.0 copy-start.5
  79.5 29.6 %all_to_all.50 = bf16[4,256,2048]{2,1,0:T(8,128)(2,1)S(1)} all-to-all(bf16[4,256,2048]{2,1,0:T(8,128)(2,1)S(1)} %broadcast_in_dim.53), channel_id=1, replica_groups={{0,4,8,12},{1,5,9,13},{2,6,10,14},{3,7,11,15},{16,17,18,19},{20,21,22,2..., dimensions={0} | all-to-all | bytes 8388608 | tf_op jit(solution)/shard_map/all_to_all | solution.py:43
  109.1 2.0 copy-done.1
  111.1 1.4 fusion.6
  112.5 6.7 %convolution_convert_fusion = bf16[1024,2048]{1,0:T(8,128)(2,1)} fusion(bf16[1024,2048]{1,0:T(8,128)(2,1)} %bitcast.33, bf16[1,224,2048]{2,1,0:T(8,128)(2,1)S(1)} %copy-done, bf16[1,2048,224]{1,2,0:T(8,128)(2,1)S(1)} %copy-done.6, f32[1024,224]{0,1:T(8,128)S(1)} %fusion.6), kind=kOutput, calls=%fused_computation | convolution fusion | flops 1882521600 | bytes 11141120 | tf_op jit(solution)/shard_map/dot_general | solution.py:125
  119.2 32.6 %all_to_all.51 = bf16[4,256,2048]{2,1,0:T(8,128)(2,1)} all-to-all(bf16[4,256,2048]{2,1,0:T(8,128)(2,1)} %bitcast.34), channel_id=1, replica_groups={{0,4,8,12},{1,5,9,13},{2,6,10,14},{3,7,11,15},{16,17,18,19},{20,21,22,2..., dimensions={0} | all-to-all | bytes 8388608 | tf_op jit(solution)/shard_map/all_to_all | solution.py:43
  151.8 3.1 %reduce_sum.77 = bf16[256,2048]{1,0:T(8,128)(2,1)S(1)} reduce(bf16[4,256,2048]{2,1,0:T(8,128)(2,1)} %all_to_all.51, bf16[]{:T(256)} %constant.104.clone.1), dimensions={0}, to_apply=%region_6.7 | reduce | flops 1572864 | bytes 5242882 | tf_op jit(solution)/shard_map/reduce_sum | solution.py:53
  154.9 12.2 %all_to_all.52 = bf16[4,64,2048]{2,1,0:T(8,128)(2,1)S(1)} all-to-all(bf16[4,64,2048]{2,1,0:T(8,128)(2,1)S(1)} %bitcast.36), channel_id=1, replica_groups={{0,1,2,3},{4,5,6,7},{8,9,10,11},{12,13,14,15},{16,20,24,28},{17,21,25,2..., dimensions={0} | all-to-all | bytes 2097152 | tf_op jit(solution)/shard_map/all_to_all | solution.py:43
  167.1 0.2 reduce_sum.78
  167.3 0.2 reshape.79
  167.5 28.9 %all_to_all.53 = bf16[32,2,2048]{2,1,0:T(2,128)(2,1)S(1)} all-to-all(bf16[32,2,2048]{2,1,0:T(2,128)(2,1)S(1)} %reshape.79), channel_id=1, replica_groups=mesh['z'=16,'c'=2,'y'=4,'x'=4] {'z','c'}, dimensions={0} | all-to-all | bytes 524288 | tf_op jit(solution)/shard_map/all_to_all | solution.py:127
  196.4 0.1 reshape.80
  196.5 0.2 fusion
  196.7 0.1 broadcast_in_dim.54
  196.8 18.4 %all_to_all.54 = bf16[16,16,2048]{2,1,0:T(8,128)(2,1)S(1)} all-to-all(bf16[16,16,2048]{2,1,0:T(8,128)(2,1)S(1)} %broadcast_in_dim.54), channel_id=1, replica_groups=mesh['z'=16,'c'=2,'y'=4,'x'=4] {'y','x'}, dimensions={0} | all-to-all | bytes 2097152 | tf_op jit(solution)/shard_map/all_to_all | solution.py:139
  215.2 1.0 copy.25
  (17 shorter events, 0.1 us)
Async XLA Ops:
  0.0 112.5 %copy-start = (bf16[1,224,2048]{2,1,0:T(8,128)(2,1)S(1)}, bf16[1,224,2048]{2,1,0:T(8,128)(2,1)}, u32[]{:S(2)}) copy-start(bf16[1,224,2048]{2,1,0:T(8,128)(2,1)} %param.19) | copy-start | bytes 2752516
  0.0 9.0 %copy-start.3 = (s32[256,2]{0,1:T(2,128)S(1)}, s32[256,2]{0,1:T(2,128)}, u32[]{:S(2)}) copy-start(s32[256,2]{0,1:T(2,128)} %param.15) | copy-start | bytes 6148
  0.0 9.1 %copy-start.4 = (f32[256,2]{0,1:T(2,128)S(1)}, f32[256,2]{0,1:T(2,128)}, u32[]{:S(2)}) copy-start(f32[256,2]{0,1:T(2,128)} %param.16) | copy-start | bytes 6148
  0.0 12.9 %copy-start.8 = (f32[128]{0:T(128)S(1)}, f32[128]{0:T(128)}, u32[]{:S(2)}) copy-start(f32[128]{0:T(128)} %param.13) | copy-start | bytes 1540
  0.0 12.9 %copy-start.7 = (bf16[512,128]{1,0:T(8,128)(2,1)S(1)}, bf16[512,128]{1,0:T(8,128)(2,1)}, u32[]{:S(2)}) copy-start(bf16[512,128]{1,0:T(8,128)(2,1)} %param.12) | copy-start | bytes 393220
  4.0 8.8 %collective-permute-start = (bf16[16,512]{1,0:T(8,128)(2,1)S(1)}, bf16[16,512]{1,0:T(8,128)(2,1)S(1)}, u32[]{:S(2)}, u32[]{:S(2)}) collective-permute-start(bf16[16,512]{1,0:T(8,128)(2,1)S(1)} %slice.69), channel_id=1, source_target_pairs={{0,16},{16,32},{32,48},{48,64},{64,80},{80,96},{96,112},{112,128},... | collective-permute-start | bytes 49160 | tf_op jit(solution)/shard_map/ppermute | solution.py:24
  12.9 12.8 %copy-start.2 = (f32[2048]{0:T(1024)S(1)}, f32[2048]{0:T(1024)}, u32[]{:S(2)}) copy-start(f32[2048]{0:T(1024)} %param.14) | copy-start | bytes 24580
  15.0 10.6 %all-to-all-start = ((bf16[16,16,128]{2,1,0:T(8,128)(2,1)}), bf16[16,16,128]{2,1,0:T(8,128)(2,1)S(1)}, u32[]{:S(2)}, u32[]{:S(2)}) async-start(bf16[16,16,128]{2,1,0:T(8,128)(2,1)} %bitcast), calls=%async_computation | async-start | bytes 131072 | tf_op jit(solution)/shard_map/all_to_all | solution.py:107
  79.5 31.6 %copy-start.5 = (bf16[1,2048,224]{1,2,0:T(8,128)(2,1)S(1)}, bf16[1,2048,224]{1,2,0:T(8,128)(2,1)}, u32[]{:S(2)}) copy-start(bf16[1,2048,224]{1,2,0:T(8,128)(2,1)} %param.17) | copy-start | bytes 2752516
  109.1 2.0 copy-start.1
  109.1 3.4 %copy-start.6 = (bf16[1,2048,224]{1,2,0:T(8,128)(2,1)S(1)}, bf16[1,2048,224]{1,2,0:T(8,128)(2,1)}, u32[]{:S(2)}) copy-start(bf16[1,2048,224]{1,2,0:T(8,128)(2,1)} %param.18) | copy-start | bytes 2752516

commit v2 on v1

v2 whole, which is shorter than its diff:
```python
import functools
import math

import jax
import jax.numpy as jnp
import numpy as np
from jax import lax
from jax.experimental import pallas as pl
from jax.experimental.pallas import tpu as pltpu
from jax.sharding import Mesh
from jax.sharding import PartitionSpec as P

GROUPS = 4
SPAN = 16
TOP_K = 2
ROWS = 16
CAP = 2
SP = ("z", "c")
TP = ("y", "x")
ALL = ("z", "c", "y", "x")

EPS = 1e-06
LANES = 128


def from_behind(value, axis, steps):
    count = lax.axis_size(axis)
    first, last = (max(0, -steps), min(count, count - steps))
    return lax.ppermute(value, axis, [(source, source + steps) for source in range(first, last)])


def plane_groups(swapped):
    sizes = [lax.axis_size(a) for a in ALL]
    index = np.arange(math.prod(sizes)).reshape(sizes)
    groups = []
    for z in range(sizes[0]):
        for c in range(sizes[1]):
            plane = index[z, c]
            groups += (plane if (c % 2 == 0) != swapped else plane.T).tolist()
    return groups


def exchange(blocks, groups):
    return lax.all_to_all(blocks, ALL, 0, 0, tiled=True, axis_index_groups=groups)


def gather_stage(block, groups):
    return exchange(jnp.broadcast_to(block[None], (len(groups[0]), *block.shape)), groups)


def sum_stage(blocks, groups):
    return jnp.sum(exchange(blocks, groups).astype(jnp.float32), axis=0).astype(jnp.bfloat16)


def expert_kernel(side, core_ref, x_ref, gain_ref, gate_ref, up_ref, down_ref, out_ref, normed):
    count, rows, lanes = x_ref.shape
    swapped = core_ref[0]

    def place(t):
        return jnp.where(swapped == 0, t, (t % side) * side + t // side)

    squares = jnp.zeros((rows, lanes), jnp.float32)
    for t in range(count):
        values = x_ref[t].astype(jnp.float32)
        squares = squares + values * values
    inverse = lax.rsqrt(jnp.sum(squares, axis=1, keepdims=True) / (count * lanes) + EPS)
    for t in range(count):
        columns = slice(t * lanes, (t + 1) * lanes)
        values = x_ref[place(t)].astype(jnp.float32)
        normed[:, columns] = (values * inverse * gain_ref[:, columns]).astype(jnp.bfloat16)
    contract = (((1,), (1,)), ((), ()))
    gate = lax.dot_general(normed[...], gate_ref[...], contract, preferred_element_type=jnp.float32)
    up = lax.dot_general(normed[...], up_ref[...], contract, preferred_element_type=jnp.float32)
    hidden = (gate * (1.0 / (1.0 + jnp.exp(-gate))) * up).astype(jnp.bfloat16)
    for t in range(0, count, 2):
        pair = jnp.dot(
            hidden,
            down_ref[:, t * lanes : (t + 2) * lanes],
            preferred_element_type=jnp.float32,
        ).astype(jnp.bfloat16)
        out_ref[place(t)] = pair[:, :lanes]
        out_ref[place(t + 1)] = pair[:, lanes:]


def expert(blocks, core, gain, gate_t, up_t, down, side, rows=256):
    count, total, lanes = blocks.shape
    units, width = gate_t.shape
    whole = lambda shape: pl.BlockSpec(shape, lambda i, core: (0, 0))
    part = pl.BlockSpec((count, rows, lanes), lambda i, core: (0, i, 0))
    return pl.pallas_call(
        functools.partial(expert_kernel, side),
        out_shape=jax.ShapeDtypeStruct(blocks.shape, jnp.bfloat16),
        grid_spec=pltpu.PrefetchScalarGridSpec(
            num_scalar_prefetch=1,
            grid=(total // rows,),
            in_specs=[
                part,
                whole((1, width)),
                whole((units, width)),
                whole((units, width)),
                whole((units, width)),
            ],
            out_specs=part,
            scratch_shapes=[pltpu.VMEM((rows, width), jnp.bfloat16)],
        ),
        compiler_params=pltpu.CompilerParams(
            dimension_semantics=("arbitrary",), vmem_limit_bytes=32 * 2**20
        ),
        cost_estimate=pl.CostEstimate(
            flops=6 * total * units * width,
            bytes_accessed=4 * total * width + 6 * units * width,
            transcendentals=total * units,
        ),
        name="expert",
    )(core, blocks, gain[None], gate_t, up_t, down)


def shards(
    residual_in,
    mix_gain,
    pool_weight,
    pool_scale,
    ffn_gain,
    route_ids,
    route_weights,
    gate_weight,
    up_weight,
    down_weight,
):
    tp_count = lax.axis_size(TP)
    sp_count = lax.axis_size(SP)
    tp_index = lax.axis_index(TP)
    sp_index = lax.axis_index(SP)
    tok_count, width = residual_in.shape
    group_width = width // GROUPS
    col_count = pool_weight.shape[1]
    slots = tok_count // ROWS * CAP
    group_index = tp_index * col_count // group_width

    rim = from_behind(residual_in[tok_count - SPAN :], SP, 1)

    def normed_group(rows):
        rows = rows.astype(jnp.float32)
        inverse = lax.rsqrt(jnp.mean(rows * rows, axis=-1, keepdims=True) + EPS)
        part = lax.dynamic_slice_in_dim(rows, group_index * group_width, group_width, 1)
        gain = lax.dynamic_slice_in_dim(mix_gain, group_index * group_width, group_width, 0)
        return (part * inverse * gain).astype(jnp.bfloat16).astype(jnp.float32)

    extended = jnp.concatenate([normed_group(rim), normed_group(residual_in)], axis=0)
    window_sum, sums = (None, extended)
    for step in range(GROUPS):
        reach = 2**step
        sums = sums[reach:] + sums[:-reach]
        here = sums[sums.shape[0] - tok_count :]
        window_sum = here if step == 0 else jnp.where(group_index == step, here, window_sum)
    window = jnp.left_shift(2, group_index)
    position = sp_index * tok_count + jnp.arange(tok_count, dtype=jnp.int32)
    divisor = jnp.minimum(position + 1, window).astype(jnp.float32)
    pooled = (window_sum / divisor[:, None] - extended[SPAN:]).astype(jnp.bfloat16)
    mixed = (jnp.dot(pooled, pool_weight, preferred_element_type=jnp.float32) * pool_scale).astype(
        jnp.bfloat16
    )
    stream = lax.dynamic_slice_in_dim(residual_in, tp_index * col_count, col_count, 1)
    after = (stream.astype(jnp.float32) + mixed.astype(jnp.float32)).astype(jnp.bfloat16)

    token = np.arange(tok_count)
    earlier = (token[:, None] // ROWS == token[None, :] // ROWS) & (token[None, :] < token[:, None])
    experts = jnp.arange(sp_count, dtype=jnp.int32)
    named = [(route_ids[:, k : k + 1] == experts[None, :]).astype(jnp.float32) for k in range(TOP_K)]
    before = jnp.dot(
        jnp.asarray(earlier, jnp.bfloat16),
        sum(named).astype(jnp.bfloat16),
        preferred_element_type=jnp.float32,
    )
    slot = jnp.arange(sp_count * slots, dtype=jnp.int32)
    block = jnp.asarray(token // ROWS * CAP, jnp.int32)
    tables = []
    for k in range(TOP_K):
        slot_of = jnp.sum(before * named[k], axis=1).astype(jnp.int32)
        target = route_ids[:, k] * slots + block + slot_of
        tables.append(target[:, None] == slot[None, :])
    outgoing = lax.dot_general(
        (tables[0] | tables[1]).astype(jnp.bfloat16),
        after,
        (((0,), (0,)), ((), ())),
        preferred_element_type=jnp.float32,
    ).astype(jnp.bfloat16)
    arrived = lax.all_to_all(outgoing.reshape(sp_count, slots, col_count), SP, 0, 0, tiled=True)
    arrived = arrived.reshape(sp_count * slots, col_count)

    first, second = (plane_groups(False), plane_groups(True))
    side = len(first[0])
    gathered = gather_stage(gather_stage(arrived, first), second)
    core = lax.axis_index("c").astype(jnp.int32).reshape(1)
    term = expert(
        gathered.reshape(tp_count, *arrived.shape),
        core,
        ffn_gain,
        gate_weight[0].T,
        up_weight[0].T,
        down_weight[0],
        side,
    )
    expert_out = sum_stage(sum_stage(term.reshape(side, side, *arrived.shape), second), first)
    returned = lax.all_to_all(
        expert_out.reshape(sp_count, slots, col_count), SP, 0, 0, tiled=True
    ).reshape(sp_count * slots, col_count)
    weights = sum(
        jnp.where(tables[k], route_weights[:, k : k + 1], 0.0) for k in range(TOP_K)
    )
    expert_mix = jnp.dot(
        weights, returned.astype(jnp.float32), precision=lax.Precision.HIGHEST
    )
    out = (after.astype(jnp.float32) + expert_mix).astype(jnp.bfloat16)
    copies = jnp.broadcast_to(out[None], (tp_count, *out.shape))
    columns = lax.all_to_all(copies, TP, 0, 0, tiled=True)
    return jnp.concatenate([columns[t] for t in range(tp_count)], axis=1)


def solution(mesh):
    torus = Mesh(mesh.devices.reshape(-1, 2, 4, mesh.shape["tp"] // 4), ALL)
    return jax.shard_map(
        shards,
        mesh=torus,
        in_specs=(
            P(SP, None),
            P(),
            P(None, TP),
            P(TP),
            P(),
            P(SP, None),
            P(SP, None),
            P(SP, None, TP),
            P(SP, None, TP),
            P(SP, TP, None),
        ),
        out_specs=P(SP, None),
        check_vma=False,
    )
```

time: 217 us -> 200 us (0.922)
  blocking collectives: 174 us -> 142 us
  waiting for transfers between devices: 9.62 us -> 21.6 us
  matrix products: 10.7 us -> 2.93 us
  Pallas kernels: 0 us -> 5.9 us
  starting transfers between devices: 8.77 us -> 13.4 us
    all_to_all x3 -> x2, blocking collectives: 87.6 us -> 54.9 us  [the longest x1 36.5 us: shards(): lax.all_to_all(outgoing.reshape(sp_count, slots, col_count), SP, 0, 0, ti...]
    all_to_all x1, waiting for transfers between devices: 6.71 us -> 21.6 us  [shards(): lax.all_to_all(expert_out.reshape(sp_count, slots, col_count), SP, 0, 0,...]
    dot_general x4 -> x3, matrix products: 8.63 us -> 1.66 us  [the longest x1 0.87 us: shards(): jnp.dot(weights, returned.astype(jnp.float32), precision=lax.Precision.HI...]
    pallas_call x0 -> x1, Pallas kernels: none -> 5.9 us  [expert(): pl.pallas_call(functools.partial(expert_kernel, side), out_shape=jax.Shap...]
    all_to_all x1, starting transfers between devices: 3.84 us -> 8.45 us  [shards(): lax.all_to_all(expert_out.reshape(sp_count, slots, col_count), SP, 0, 0,...]
    ppermute x1, waiting for transfers between devices: 2.92 us -> 0.01 us  [from_behind(): lax.ppermute(value, axis, [(source, source + steps) for source in range(f...]
    reduce_sum x6 -> x4, other arithmetic: 5.26 us -> 5.53 us  [the longest x2 3.89 us: sum_stage(): jnp.sum(exchange(blocks, groups).astype(jnp.float32), axis=0)]
  transfers between devices with their start and end apart: 2 -> 2, of which waited for: 2 -> 1; matrix products, arithmetic and copies ran while one was open for 0% -> 2% of each run, Pallas kernels for 0% -> 0%
where the time goes in v2:
time: 200 us; the launch traced here: 199 us
  blocking collectives  142 us (71%)
  waiting for transfers between devices  21.6 us (11%)
  starting transfers between devices  13.4 us (7%)
  other arithmetic  7.44 us (4%)
  Pallas kernels  5.9 us (3%)
  local copies, waits for them, and re-layouts  4.86 us (2%)
  matrix products  2.93 us (1%)
    all_to_all x4, blocking collectives, exchange(): lax.all_to_all(blocks, ALL, 0, 0, tiled=True, axis_index_groups=groups)  87.5 us
    all_to_all x1, blocking collectives, shards(): lax.all_to_all(outgoing.reshape(sp_count, slots, col_count), SP, 0, 0, ti...  36.5 us
    all_to_all x1, waiting for transfers between devices, shards(): lax.all_to_all(expert_out.reshape(sp_count, slots, col_count), SP, 0, 0,...  21.6 us
    all_to_all x1, blocking collectives, shards(): columns = lax.all_to_all(copies, TP, 0, 0, tiled=True)  18.4 us
    all_to_all x1, starting transfers between devices, shards(): lax.all_to_all(expert_out.reshape(sp_count, slots, col_count), SP, 0, 0,...  8.45 us
    pallas_call x1, Pallas kernels, expert(): pl.pallas_call(functools.partial(expert_kernel, side), out_shape=jax.Shap...  5.9 us
    ppermute x1, starting transfers between devices, from_behind(): lax.ppermute(value, axis, [(source, source + steps) for source in range(f...  4.91 us
  transfers between devices with their start and end apart: 2, of which 1 were waited for; matrix products, arithmetic and copies ran while one was open for 2% of the time, Pallas kernels for 0%

profile of v2, /device:TPU:1, one launch (start us, length us, event | category | flops | bytes accessed | tf_op | source)
XLA Modules:
  0.0 198.9 jit_solution(10016602603985131359)
XLA Ops:
  0.0 0.0 copy-start
  0.0 0.0 copy-start.6
  0.0 0.9 slice.101
  0.9 4.9 %collective-permute-start = (bf16[16,2048]{1,0:T(8,128)(2,1)S(1)}, bf16[16,2048]{1,0:T(8,128)(2,1)S(1)}, u32[]{:S(2)}, u32[]{:S(2)}) collective-permute-start(bf16[16,2048]{1,0:T(8,128)(2,1)S(1)} %slice.101), channel_id=1, source_target_pairs={{0,16},{16,32},{32,48},{48,64},{64,80},{80,96},{96,112},{112,128},... | collective-permute-start | bytes 196616 | tf_op jit(solution)/shard_map/ppermute | solution.py:29
  5.9 1.5 convert_element_type.74
  7.3 1.5 multiply_reduce_fusion
  8.9 0.0 copy-done.6
  8.9 0.8 dynamic_slice.15
  9.7 0.1 fusion.23
  9.8 0.0 copy-done.10
  9.8 0.2 select_reduce_fusion.1
  10.0 0.0 copy-done.8
  10.1 0.0 collective-permute-done
  10.1 0.1 multiply_reduce_fusion.1
  10.2 0.1 fusion.41
  10.3 0.1 fusion.10
  10.4 0.1 slice_add_fusion.1
  10.5 0.1 slice_add_fusion
  10.5 0.1 fusion.44
  10.7 0.0 copy-done
  10.7 0.0 copy-done.9
  10.7 1.3 fusion.4
  12.0 0.6 convolution_convert_fusion
  12.6 36.5 %all_to_all.35 = bf16[32,32,128]{2,1,0:T(8,128)(2,1)S(1)} all-to-all(bf16[32,32,128]{2,1,0:T(8,128)(2,1)S(1)} %bitcast.95), channel_id=1, replica_groups=mesh['z'=16,'c'=2,'y'=4,'x'=4] {'z','c'}, dimensions={0} | all-to-all | bytes 524288 | tf_op jit(solution)/shard_map/all_to_all | solution.py:188
  49.1 0.1 broadcast_in_dim.62
  49.2 13.8 %all_to_all.36 = bf16[4,1024,128]{2,1,0:T(8,128)(2,1)S(1)} all-to-all(bf16[4,1024,128]{2,1,0:T(8,128)(2,1)S(1)} %broadcast_in_dim.62), channel_id=1, replica_groups={{0,1,2,3},{4,5,6,7},{8,9,10,11},{12,13,14,15},{16,20,24,28},{17,21,25,2..., dimensions={0} | all-to-all | bytes 2097152 | tf_op jit(solution)/shard_map/all_to_all | solution.py:44
  63.1 0.8 broadcast_in_dim.63
  63.9 0.0 copy-start.1
  63.9 0.0 copy-start.2
  63.9 0.0 copy-start.3
  63.9 0.0 copy-start.4
  63.9 30.8 %all_to_all.37 = bf16[4,4,1024,128]{3,2,1,0:T(8,128)(2,1)S(1)} all-to-all(bf16[4,4,1024,128]{3,2,1,0:T(8,128)(2,1)S(1)} %broadcast_in_dim.63), channel_id=1, replica_groups={{0,4,8,12},{1,5,9,13},{2,6,10,14},{3,7,11,15},{16,17,18,19},{20,21,22,2..., dimensions={0} | all-to-all | bytes 8388608 | tf_op jit(solution)/shard_map/all_to_all | solution.py:44
  94.8 0.0 copy-done.1
  94.8 0.0 copy-done.2
  94.8 0.0 copy-done.3
  94.8 5.9 %expert.1 = bf16[16,1024,128]{2,1,0:T(8,128)(2,1)S(1)} custom-call(s32[1]{0:T(128)} %bitcast.4.core_ref, bf16[16,1024,128]{2,1,0:T(8,128)(2,1)S(1)} %bitcast.87, f32[1,2048]{1,0:T(1,128)S(1)} %bitcast.92, bf16[224,2048]{1,0:T(8,128)(2,1)S(1)} %bitcast.89, bf16[224,2048]{1,0:T(8,128)(2,1)S(1)} %bitcast.90, bf16[224,2048]{1,0:T(8,128)(2,1)S(1)} %bitcast.91), custom_call_target="tpu_custom_call" | custom-call | flops 2818572288 | bytes 11141120 | tf_op jit(solution)/shard_map/expert/pallas_call | solution.py:90
  100.7 30.3 %all_to_all.38 = bf16[4,4,1024,128]{3,2,1,0:T(8,128)(2,1)} all-to-all(bf16[4,4,1024,128]{3,2,1,0:T(8,128)(2,1)S(1)} %bitcast.88), channel_id=1, replica_groups={{0,4,8,12},{1,5,9,13},{2,6,10,14},{3,7,11,15},{16,17,18,19},{20,21,22,2..., dimensions={0} | all-to-all | bytes 8388608 | tf_op jit(solution)/shard_map/all_to_all | solution.py:44
  131.0 3.0 %reduce_sum.64 = bf16[4,1024,128]{2,1,0:T(8,128)(2,1)S(1)} reduce(bf16[4,4,1024,128]{3,2,1,0:T(8,128)(2,1)} %all_to_all.38, bf16[]{:T(256)} %constant.70.clone.1), dimensions={0}, to_apply=%region_4.5 | reduce | flops 1572864 | bytes 5242882 | tf_op jit(solution)/shard_map/reduce_sum | solution.py:52
  134.0 12.5 %all_to_all.39 = bf16[4,1024,128]{2,1,0:T(8,128)(2,1)S(1)} all-to-all(bf16[4,1024,128]{2,1,0:T(8,128)(2,1)S(1)} %reduce_sum.64), channel_id=1, replica_groups={{0,1,2,3},{4,5,6,7},{8,9,10,11},{12,13,14,15},{16,20,24,28},{17,21,25,2..., dimensions={0} | all-to-all | bytes 2097152 | tf_op jit(solution)/shard_map/all_to_all | solution.py:44
  146.5 0.9 reduce_sum.65
  147.4 8.5 %all-to-all-start.5 = ((bf16[32,32,128]{2,1,0:T(8,128)(2,1)}), bf16[32,32,128]{2,1,0:T(8,128)(2,1)S(1)}, u32[]{:S(2)}, u32[]{:S(2)}) async-start(bf16[32,32,128]{2,1,0:T(8,128)(2,1)} %bitcast.15), calls=%async_computation.5 | async-start | bytes 524288 | tf_op jit(solution)/shard_map/all_to_all | solution.py:205
  155.9 21.6 %all-to-all-done.5 = bf16[32,32,128]{2,1,0:T(8,128)(2,1)S(1)} async-done(((bf16[32,32,128]{2,1,0:T(8,128)(2,1)}), bf16[32,32,128]{2,1,0:T(8,128)(2,1)S(1)}, u32[]{:S(2)}, u32[]{:S(2)}) %all-to-all-start.5) | async-done | bytes 262176 | tf_op jit(solution)/shard_map/all_to_all | solution.py:205
  177.5 0.9 fusion
  178.4 0.2 broadcast_in_dim.65
  178.6 18.4 %all_to_all.40 = bf16[16,256,128]{2,1,0:T(8,128)(2,1)S(1)} all-to-all(bf16[16,256,128]{2,1,0:T(8,128)(2,1)S(1)} %broadcast_in_dim.65), channel_id=1, replica_groups=mesh['z'=16,'c'=2,'y'=4,'x'=4] {'y','x'}, dimensions={0} | all-to-all | bytes 2097152 | tf_op jit(solution)/shard_map/all_to_all | solution.py:216
  197.3 0.0 copy-start.5
  197.3 1.0 copy-done.5
  198.3 0.6 fusion.25
  (28 shorter events, 0.4 us)
Async XLA Ops:
  0.0 10.7 %copy-start = (bf16[512,128]{1,0:T(8,128)(2,1)S(1)}, bf16[512,128]{1,0:T(8,128)(2,1)}, u32[]{:S(2)}) copy-start(bf16[512,128]{1,0:T(8,128)(2,1)} %param.14) | copy-start | bytes 393220
  0.0 9.8 %copy-start.10 = (bf16[256,256]{1,0:T(8,128)(2,1)S(1)}, bf16[256,256]{1,0:T(8,128)(2,1)}, u32[]{:S(2)}) copy-start(bf16[256,256]{1,0:T(8,128)(2,1)} %constant.71.clone) | copy-start | bytes 393220
  0.0 10.0 %copy-start.8 = (s32[256]{0:T(256)S(1)}, s32[256]{0:T(256)}, u32[]{:S(2)}) copy-start(s32[256]{0:T(256)} %constant.72.clone) | copy-start | bytes 3076
  0.0 8.9 %copy-start.6 = (s32[256,2]{0,1:T(2,128)S(1)}, s32[256,2]{0,1:T(2,128)}, u32[]{:S(2)}) copy-start(s32[256,2]{0,1:T(2,128)} %param.17) | copy-start | bytes 6148
  0.9 9.1 %collective-permute-start = (bf16[16,2048]{1,0:T(8,128)(2,1)S(1)}, bf16[16,2048]{1,0:T(8,128)(2,1)S(1)}, u32[]{:S(2)}, u32[]{:S(2)}) collective-permute-start(bf16[16,2048]{1,0:T(8,128)(2,1)S(1)} %slice.101), channel_id=1, source_target_pairs={{0,16},{16,32},{32,48},{48,64},{64,80},{80,96},{96,112},{112,128},... | collective-permute-start | bytes 196616 | tf_op jit(solution)/shard_map/ppermute | solution.py:29
  8.8 1.9 copy-start.9
  63.9 30.9 %copy-start.1 = (bf16[1,2048,224]{1,2,0:T(8,128)(2,1)S(1)}, bf16[1,2048,224]{1,2,0:T(8,128)(2,1)}, u32[]{:S(2)}) copy-start(bf16[1,2048,224]{1,2,0:T(8,128)(2,1)} %param.19) | copy-start | bytes 2752516
  63.9 30.9 %copy-start.2 = (bf16[1,2048,224]{1,2,0:T(8,128)(2,1)S(1)}, bf16[1,2048,224]{1,2,0:T(8,128)(2,1)}, u32[]{:S(2)}) copy-start(bf16[1,2048,224]{1,2,0:T(8,128)(2,1)} %param.20) | copy-start | bytes 2752516
  63.9 30.9 %copy-start.3 = (bf16[1,224,2048]{2,1,0:T(8,128)(2,1)S(1)}, bf16[1,224,2048]{2,1,0:T(8,128)(2,1)}, u32[]{:S(2)}) copy-start(bf16[1,224,2048]{2,1,0:T(8,128)(2,1)} %param.21) | copy-start | bytes 2752516
  63.9 30.9 %copy-start.4 = (f32[2048]{0:T(1024)S(1)}, f32[2048]{0:T(1024)}, u32[]{:S(2)}) copy-start(f32[2048]{0:T(1024)} %param.16) | copy-start | bytes 24580
  131.0 24.8 %copy-start.7 = (f32[256,2]{0,1:T(2,128)S(1)}, f32[256,2]{0,1:T(2,128)}, u32[]{:S(2)}) copy-start(f32[256,2]{0,1:T(2,128)} %param.18) | copy-start | bytes 6148
  147.4 30.1 %all-to-all-start.5 = ((bf16[32,32,128]{2,1,0:T(8,128)(2,1)}), bf16[32,32,128]{2,1,0:T(8,128)(2,1)S(1)}, u32[]{:S(2)}, u32[]{:S(2)}) async-start(bf16[32,32,128]{2,1,0:T(8,128)(2,1)} %bitcast.15), calls=%async_computation.5 | async-start | bytes 524288 | tf_op jit(solution)/shard_map/all_to_all | solution.py:205
  197.3 1.0 copy-start.5

commit v3 on v2

v3 whole, which is shorter than its diff:
```python
import functools
import math

import jax
import jax.numpy as jnp
import numpy as np
from jax import lax
from jax.experimental import pallas as pl
from jax.experimental.pallas import tpu as pltpu
from jax.sharding import Mesh
from jax.sharding import PartitionSpec as P

GROUPS = 4
SPAN = 16
TOP_K = 2
ROWS = 16
CAP = 2
SP = ("z", "c")
TP = ("y", "x")
ALL = ("z", "c", "y", "x")

EPS = 1e-06
LANES = 128


def from_behind(value, axis, steps):
    count = lax.axis_size(axis)
    first, last = (max(0, -steps), min(count, count - steps))
    return lax.ppermute(value, axis, [(source, source + steps) for source in range(first, last)])


def planes():
    sizes = [lax.axis_size(a) for a in ALL]
    index = np.arange(math.prod(sizes)).reshape(sizes)
    return [
        index[z, c] if c % 2 == 0 else index[z, c].T
        for z in range(sizes[0])
        for c in range(sizes[1])
    ]


def from_quad(value, steps):
    pairs = []
    for plane in planes():
        pairs += list(zip(plane.ravel().tolist(), np.roll(plane, -steps, axis=1).ravel().tolist()))
    return lax.ppermute(value, ALL, pairs)


def exchange(blocks):
    groups = [plane.ravel().tolist() for plane in planes()]
    return lax.all_to_all(blocks, ALL, 0, 0, tiled=True, axis_index_groups=groups)


def place(t, side, swapped):
    return jnp.where(swapped == 0, t, (t % side) * side + t // side)


def norm_kernel(side, core_ref, x_ref, gain_ref, normed_ref):
    count, rows, lanes = x_ref.shape
    squares = jnp.zeros((rows, lanes), jnp.float32)
    for t in range(count):
        values = x_ref[t].astype(jnp.float32)
        squares = squares + values * values
    inverse = lax.rsqrt(jnp.sum(squares, axis=1, keepdims=True) / (count * lanes) + EPS)
    for t in range(count):
        columns = slice(t * lanes, (t + 1) * lanes)
        values = x_ref[place(t, side, core_ref[0])].astype(jnp.float32)
        normed_ref[:, columns] = (values * inverse * gain_ref[:, columns]).astype(jnp.bfloat16)


def expert_kernel(side, parts, core_ref, normed_ref, *refs):
    weight_refs, refs = (refs[:parts], refs[parts:])
    last = len(refs[-1].shape) == 3
    total_refs, out_ref = (refs[:-1], refs[-1])
    width = normed_ref.shape[1]
    units = weight_refs[0].shape[0] // 3
    contract = (((1,), (1,)), ((), ()))
    normed = normed_ref[...]
    hidden = []
    for ref in weight_refs:
        gate = lax.dot_general(normed, ref[:units], contract, preferred_element_type=jnp.float32)
        up = lax.dot_general(
            normed, ref[units : 2 * units], contract, preferred_element_type=jnp.float32
        )
        hidden.append((gate * (1.0 / (1.0 + jnp.exp(-gate))) * up).astype(jnp.bfloat16))
    step = 2 * LANES
    for first in range(0, width, step):
        columns = slice(first, first + step)
        total = 0.0
        for part, ref in zip(hidden, weight_refs):
            total = total + jnp.dot(
                part, ref[2 * units :, columns], preferred_element_type=jnp.float32
            )
        for ref in total_refs:
            total = total + ref[:, columns]
        if last:
            for half in range(2):
                t = first // LANES + half
                out_ref[place(t, side, core_ref[0])] = total[
                    :, half * LANES : (half + 1) * LANES
                ].astype(jnp.bfloat16)
        else:
            out_ref[:, columns] = total


SCALARS = pl.BlockSpec(memory_space=pltpu.SMEM)
VECTORS = pl.BlockSpec(memory_space=pltpu.VMEM)


def norm_rows(blocks, core, gain, side):
    count, rows, lanes = blocks.shape
    return pl.pallas_call(
        functools.partial(norm_kernel, side),
        out_shape=jax.ShapeDtypeStruct((rows, count * lanes), jnp.bfloat16),
        in_specs=[SCALARS, VECTORS, VECTORS],
        out_specs=VECTORS,
        cost_estimate=pl.CostEstimate(
            flops=4 * blocks.size, bytes_accessed=4 * blocks.size, transcendentals=rows
        ),
        name="norm",
    )(core, blocks, gain[None])


def expert(normed, core, weights, totals, side, last):
    rows, width = normed.shape
    units = weights[0].shape[0] // 3
    if last:
        out = jax.ShapeDtypeStruct((width // LANES, rows, LANES), jnp.bfloat16)
    else:
        out = jax.ShapeDtypeStruct((rows, width), jnp.float32)
    return pl.pallas_call(
        functools.partial(expert_kernel, side, len(weights)),
        out_shape=out,
        in_specs=[SCALARS] + [VECTORS] * (1 + len(weights) + len(totals)),
        out_specs=VECTORS,
        compiler_params=pltpu.CompilerParams(vmem_limit_bytes=40 * 2**20),
        cost_estimate=pl.CostEstimate(
            flops=6 * rows * units * width * len(weights),
            bytes_accessed=6 * units * width * len(weights),
            transcendentals=rows * units * len(weights),
        ),
        name="expert",
    )(core, normed, *weights, *totals)


def assemble_kernel(columns_ref, out_ref):
    for t in range(columns_ref.shape[0]):
        out_ref[:, t * LANES : (t + 1) * LANES] = columns_ref[t]


def assemble(columns, rows=64):
    count, total, lanes = columns.shape
    return pl.pallas_call(
        assemble_kernel,
        out_shape=jax.ShapeDtypeStruct((total, count * lanes), columns.dtype),
        grid=(total // rows,),
        in_specs=[pl.BlockSpec((count, rows, lanes), lambda i: (0, i, 0))],
        out_specs=pl.BlockSpec((rows, count * lanes), lambda i: (i, 0)),
        name="assemble",
    )(columns)


def shards(
    residual_in,
    mix_gain,
    pool_weight,
    pool_scale,
    ffn_gain,
    route_ids,
    route_weights,
    gate_weight,
    up_weight,
    down_weight,
):
    tp_count = lax.axis_size(TP)
    sp_count = lax.axis_size(SP)
    tp_index = lax.axis_index(TP)
    sp_index = lax.axis_index(SP)
    tok_count, width = residual_in.shape
    group_width = width // GROUPS
    col_count = pool_weight.shape[1]
    slots = tok_count // ROWS * CAP
    group_index = tp_index * col_count // group_width

    own = jnp.concatenate([gate_weight[0].T, up_weight[0].T, down_weight[0]], axis=0)
    others = [from_quad(own, steps) for steps in (1, -1, 2)]
    rim = from_behind(residual_in[tok_count - SPAN :], SP, 1)

    def normed_group(rows):
        rows = rows.astype(jnp.float32)
        inverse = lax.rsqrt(jnp.mean(rows * rows, axis=-1, keepdims=True) + EPS)
        part = lax.dynamic_slice_in_dim(rows, group_index * group_width, group_width, 1)
        gain = lax.dynamic_slice_in_dim(mix_gain, group_index * group_width, group_width, 0)
        return lax.reduce_precision(part * inverse * gain, 8, 7)

    extended = jnp.concatenate([normed_group(rim), normed_group(residual_in)], axis=0)
    window_sum, sums = (None, extended)
    for step in range(GROUPS):
        reach = 2**step
        sums = sums[reach:] + sums[:-reach]
        here = sums[sums.shape[0] - tok_count :]
        window_sum = here if step == 0 else jnp.where(group_index == step, here, window_sum)
    window = jnp.left_shift(2, group_index)
    position = sp_index * tok_count + jnp.arange(tok_count, dtype=jnp.int32)
    divisor = jnp.minimum(position + 1, window).astype(jnp.float32)
    pooled = (window_sum / divisor[:, None] - extended[SPAN:]).astype(jnp.bfloat16)
    mixed = (jnp.dot(pooled, pool_weight, preferred_element_type=jnp.float32) * pool_scale).astype(
        jnp.bfloat16
    )
    stream = lax.dynamic_slice_in_dim(residual_in, tp_index * col_count, col_count, 1)
    after = (stream.astype(jnp.float32) + mixed.astype(jnp.float32)).astype(jnp.bfloat16)

    token = np.arange(tok_count)
    earlier = (token[:, None] // ROWS == token[None, :] // ROWS) & (token[None, :] < token[:, None])
    experts = jnp.arange(sp_count, dtype=jnp.int32)
    named = [(route_ids[:, k : k + 1] == experts[None, :]).astype(jnp.float32) for k in range(TOP_K)]
    before = jnp.dot(
        jnp.asarray(earlier, jnp.bfloat16),
        sum(named).astype(jnp.bfloat16),
        preferred_element_type=jnp.float32,
    )
    slot = jnp.arange(sp_count * slots, dtype=jnp.int32)
    block = jnp.asarray(token // ROWS * CAP, jnp.int32)
    tables = []
    for k in range(TOP_K):
        slot_of = jnp.sum(before * named[k], axis=1).astype(jnp.int32)
        target = route_ids[:, k] * slots + block + slot_of
        tables.append(target[:, None] == slot[None, :])
    outgoing = lax.dot_general(
        (tables[0] | tables[1]).astype(jnp.bfloat16),
        after,
        (((0,), (0,)), ((), ())),
        preferred_element_type=jnp.float32,
    ).astype(jnp.bfloat16)
    arrived = lax.all_to_all(outgoing.reshape(sp_count, slots, col_count), SP, 0, 0, tiled=True)
    arrived = arrived.reshape(sp_count * slots, col_count)

    side = lax.axis_size("x")
    core = lax.axis_index("c").astype(jnp.int32).reshape(1)
    quarter = arrived.reshape(1, side, -1, col_count)
    quarter = jnp.broadcast_to(quarter, (side, *quarter.shape[1:]))
    gathered = exchange(quarter.reshape(tp_count, -1, col_count))
    normed = norm_rows(gathered, core, ffn_gain, side)
    total = expert(normed, core, [own, *others[:2]], [], side, False)
    term = expert(normed, core, others[2:], [total], side, True)
    summed = exchange(term).reshape(quarter.shape)
    expert_out = jnp.sum(summed.astype(jnp.float32), axis=0).astype(jnp.bfloat16)
    returned = lax.all_to_all(
        expert_out.reshape(sp_count, slots, col_count), SP, 0, 0, tiled=True
    ).reshape(sp_count * slots, col_count)
    weights = sum(
        jnp.where(tables[k], route_weights[:, k : k + 1], 0.0) for k in range(TOP_K)
    )
    expert_mix = jnp.dot(
        weights, returned.astype(jnp.float32), precision=lax.Precision.HIGHEST
    )
    out = (after.astype(jnp.float32) + expert_mix).astype(jnp.bfloat16)
    copies = jnp.broadcast_to(out[None], (tp_count, *out.shape))
    columns = lax.all_to_all(copies, TP, 0, 0, tiled=True)
    return assemble(columns)


def solution(mesh):
    torus = Mesh(mesh.devices.reshape(-1, 2, 4, mesh.shape["tp"] // 4), ALL)
    return jax.shard_map(
        shards,
        mesh=torus,
        in_specs=(
            P(SP, None),
            P(),
            P(None, TP),
            P(TP),
            P(),
            P(SP, None),
            P(SP, None),
            P(SP, None, TP),
            P(SP, None, TP),
            P(SP, TP, None),
        ),
        out_specs=P(SP, None),
        check_vma=False,
    )
```

time: 200 us -> 183 us (0.915)
  blocking collectives: 142 us -> 97.9 us
  starting transfers between devices: 13.4 us -> 32.6 us
  Pallas kernels: 5.9 us -> 14.3 us
    all_to_all x4 -> x2, blocking collectives: 87.5 us -> 41.8 us  [exchange(): lax.all_to_all(blocks, ALL, 0, 0, tiled=True, axis_index_groups=groups)]
    ppermute x0 -> x3, starting transfers between devices: none -> 11.1 us  [from_quad(): return lax.ppermute(value, ALL, pairs)]
    all_to_all x1, starting transfers between devices: 8.45 us -> 16.8 us  [shards(): lax.all_to_all(expert_out.reshape(sp_count, slots, col_count), SP, 0, 0,...]
    pallas_call x1 -> x4, Pallas kernels: 5.9 us -> 14.3 us  [the longest x2 8.14 us: expert(): pl.pallas_call(functools.partial(expert_kernel, side, len(weights)), out_...]
    reduce_sum x2 -> x1, other arithmetic: 3.89 us -> 0.91 us  [shards(): jnp.sum(summed.astype(jnp.float32), axis=0).astype(jnp.bfloat16)]
    concatenate x0 -> x1, other arithmetic: none -> 2.11 us  [shards(): jnp.concatenate([gate_weight[0].T, up_weight[0].T, down_weight[0]], axis=0)]
  transfers between devices with their start and end apart: 2 -> 5, of which waited for: 1 -> 1; matrix products, arithmetic and copies ran while one was open for 2% -> 5% of each run, Pallas kernels for 0% -> 4%
where the time goes in v3:
time: 183 us; the launch traced here: 182 us
  blocking collectives  97.9 us (53%)
  starting transfers between devices  32.6 us (18%)
  waiting for transfers between devices  22.2 us (12%)
  Pallas kernels  14.3 us (8%)
  other arithmetic  7.89 us (4%)
  local copies, waits for them, and re-layouts  3.75 us (2%)
  matrix products  2.92 us (2%)
    all_to_all x2, blocking collectives, exchange(): lax.all_to_all(blocks, ALL, 0, 0, tiled=True, axis_index_groups=groups)  41.8 us
    all_to_all x1, blocking collectives, shards(): lax.all_to_all(outgoing.reshape(sp_count, slots, col_count), SP, 0, 0, ti...  36.5 us
    all_to_all x1, waiting for transfers between devices, shards(): lax.all_to_all(expert_out.reshape(sp_count, slots, col_count), SP, 0, 0,...  22.2 us
    all_to_all x1, blocking collectives, shards(): columns = lax.all_to_all(copies, TP, 0, 0, tiled=True)  19.6 us
    all_to_all x1, starting transfers between devices, shards(): lax.all_to_all(expert_out.reshape(sp_count, slots, col_count), SP, 0, 0,...  16.8 us
    ppermute x3, starting transfers between devices, from_quad(): return lax.ppermute(value, ALL, pairs)  11.1 us
    pallas_call x2, Pallas kernels, expert(): pl.pallas_call(functools.partial(expert_kernel, side, len(weights)), out_...  8.14 us
    ppermute x1, starting transfers between devices, from_behind(): lax.ppermute(value, axis, [(source, source + steps) for source in range(f...  4.76 us
  transfers between devices with their start and end apart: 5, of which 1 were waited for; matrix products, arithmetic and copies ran while one was open for 5% of the time, Pallas kernels for 4%

profile of v3, /device:TPU:1, one launch (start us, length us, event | category | flops | bytes accessed | tf_op | source)
XLA Modules:
  0.0 182.0 jit_solution(18411938480901324437)
XLA Ops:
  0.0 2.1 %pad_maximum_fusion.refs_0_ = bf16[672,2048]{1,0:T(8,128)(2,1)S(1)} fusion(bf16[224,2048]{1,0:T(8,128)(2,1)} %bitcast.26, bf16[224,2048]{1,0:T(8,128)(2,1)} %bitcast.27, bf16[224,2048]{1,0:T(8,128)(2,1)} %bitcast.28), kind=kLoop, calls=%fused_computation | loop fusion | flops 8257536 | bytes 5505024 | tf_op jit(solution)/shard_map/concatenate | solution.py:185
  2.1 0.0 copy-start.3
  2.1 0.0 copy-start.7
  2.1 4.2 %collective-permute-start.2 = (bf16[672,2048]{1,0:T(8,128)(2,1)S(1)}, bf16[672,2048]{1,0:T(8,128)(2,1)}, u32[]{:S(2)}, u32[]{:S(2)}) collective-permute-start(bf16[672,2048]{1,0:T(8,128)(2,1)S(1)} %pad_maximum_fusion.refs_0_), channel_id=1, source_target_pairs={{0,1},{1,2},{2,3},{3,0},{4,5},{5,6},{6,7},{7,4},{8,9},{9,10},{10,1... | collective-permute-start | bytes 8257544 | tf_op jit(solution)/shard_map/ppermute | solution.py:46
  6.3 3.4 %collective-permute-start.3 = (bf16[672,2048]{1,0:T(8,128)(2,1)S(1)}, bf16[672,2048]{1,0:T(8,128)(2,1)}, u32[]{:S(2)}, u32[]{:S(2)}) collective-permute-start(bf16[672,2048]{1,0:T(8,128)(2,1)S(1)} %pad_maximum_fusion.refs_0_), channel_id=1, source_target_pairs={{0,3},{1,0},{2,1},{3,2},{4,7},{5,4},{6,5},{7,6},{8,11},{9,8},{10,9... | collective-permute-start | bytes 8257544 | tf_op jit(solution)/shard_map/ppermute | solution.py:46
  9.7 3.5 %collective-permute-start.1 = (bf16[672,2048]{1,0:T(8,128)(2,1)S(1)}, bf16[672,2048]{1,0:T(8,128)(2,1)}, u32[]{:S(2)}, u32[]{:S(2)}) collective-permute-start(bf16[672,2048]{1,0:T(8,128)(2,1)S(1)} %pad_maximum_fusion.refs_0_), channel_id=1, source_target_pairs={{0,2},{1,3},{2,0},{3,1},{4,6},{5,7},{6,4},{7,5},{8,10},{9,11},{10,... | collective-permute-start | bytes 8257544 | tf_op jit(solution)/shard_map/ppermute | solution.py:46
  13.2 0.8 slice.53
  14.1 4.8 %collective-permute-start = (bf16[16,2048]{1,0:T(8,128)(2,1)S(1)}, bf16[16,2048]{1,0:T(8,128)(2,1)S(1)}, u32[]{:S(2)}, u32[]{:S(2)}) collective-permute-start(bf16[16,2048]{1,0:T(8,128)(2,1)S(1)} %slice.53), channel_id=1, source_target_pairs={{0,16},{16,32},{32,48},{48,64},{64,80},{80,96},{96,112},{112,128},... | collective-permute-start | bytes 196616 | tf_op jit(solution)/shard_map/ppermute | solution.py:29
  18.9 0.0 copy-start.2
  18.9 0.0 copy-start.5
  18.9 3.0 %convert_element_type.58 = f32[256,2048]{1,0:T(8,128)} convert(bf16[256,2048]{1,0:T(8,128)(2,1)} %param.12) | non-fusion elementwise | flops 524288 | bytes 3145728 | tf_op jit(solution)/shard_map/convert_element_type | solution.py:190
  21.8 0.0 copy-done.2
  21.8 0.3 multiply_reduce_fusion
  22.2 0.8 dynamic_slice.15
  23.0 1.2 multiply_reduce-precision_fusion
  24.1 0.0 copy-done.7
  24.1 0.2 select_reduce_fusion.1
  24.3 0.0 copy-done.5
  24.4 0.0 collective-permute-done
  24.4 0.1 multiply_reduce_fusion.1
  24.6 0.1 multiply_reduce-precision_fusion.1
  24.6 0.1 fusion.10
  24.7 0.0 copy-start.6
  24.7 0.1 slice_add_fusion.1
  24.8 0.1 slice_add_fusion
  24.9 0.1 fusion.26
  25.0 0.4 copy-done.6
  25.4 1.3 fusion.4
  26.7 0.6 convolution_convert_fusion
  27.3 36.5 %all_to_all.25 = bf16[32,32,128]{2,1,0:T(8,128)(2,1)S(1)} all-to-all(bf16[32,32,128]{2,1,0:T(8,128)(2,1)S(1)} %bitcast.30), channel_id=1, replica_groups=mesh['z'=16,'c'=2,'y'=4,'x'=4] {'z','c'}, dimensions={0} | all-to-all | bytes 524288 | tf_op jit(solution)/shard_map/all_to_all | solution.py:235
  63.8 0.2 broadcast_in_dim.56
  64.0 21.9 %all_to_all.26.x_ref = bf16[16,256,128]{2,1,0:T(8,128)(2,1)} all-to-all(bf16[16,256,128]{2,1,0:T(8,128)(2,1)S(1)} %bitcast.23), channel_id=1, replica_groups={{0,1,2,3,4,5,6,7,8,9,10,11,12,13,14,15},{16,20,24,28,17,21,25,29,18,22,..., dimensions={0} | all-to-all | bytes 2097152 | tf_op jit(solution)/shard_map/all_to_all | solution.py:51
  85.9 2.7 %norm.1.normed_ref = bf16[256,2048]{1,0:T(8,128)(2,1)} custom-call(s32[1]{0:T(128)} %bitcast.4.core_ref, bf16[16,256,128]{2,1,0:T(8,128)(2,1)} %all_to_all.26.x_ref, f32[1,2048]{1,0:T(1,128)} %bitcast.31), custom_call_target="tpu_custom_call" | custom-call | flops 2097152 | bytes 2097152 | tf_op jit(solution)/shard_map/norm/pallas_call | solution.py:112
  88.6 0.0 collective-permute-done.2.refs_1_
  88.6 0.0 collective-permute-done.3.refs_2_
  88.6 1.2 copy-done.1
  89.8 5.2 %expert.2.refs_1_ = f32[256,2048]{1,0:T(8,128)S(1)} custom-call(s32[1]{0:T(128)} %bitcast.4.core_ref, bf16[256,2048]{1,0:T(8,128)(2,1)S(1)} %copy-done.1, bf16[672,2048]{1,0:T(8,128)(2,1)S(1)} %pad_maximum_fusion.refs_0_, bf16[672,2048]{1,0:T(8,128)(2,1)} %collective-permute-done.2.refs_1_, bf16[672,2048]{1,0:T(8,128)(2,1)} %collective-permute-done.3.refs_2_), custom_call_target="tpu_custom_call" | custom-call | flops 2113929216 | bytes 8257536 | tf_op jit(solution)/shard_map/expert/pallas_call | solution.py:131
  95.1 0.0 collective-permute-done.1.refs_0_
  95.1 2.9 %expert.3 = bf16[16,256,128]{2,1,0:T(8,128)(2,1)S(1)} custom-call(s32[1]{0:T(128)} %bitcast.4.core_ref, bf16[256,2048]{1,0:T(8,128)(2,1)S(1)} %copy-done.1, bf16[672,2048]{1,0:T(8,128)(2,1)} %collective-permute-done.1.refs_0_, f32[256,2048]{1,0:T(8,128)S(1)} %expert.2.refs_1_), custom_call_target="tpu_custom_call" | custom-call | flops 704643072 | bytes 2752512 | tf_op jit(solution)/shard_map/expert/pallas_call | solution.py:131
  98.0 0.0 copy-start.4
  98.0 19.8 %all_to_all.27 = bf16[16,256,128]{2,1,0:T(8,128)(2,1)S(1)} all-to-all(bf16[16,256,128]{2,1,0:T(8,128)(2,1)S(1)} %expert.3), channel_id=1, replica_groups={{0,1,2,3,4,5,6,7,8,9,10,11,12,13,14,15},{16,20,24,28,17,21,25,29,18,22,..., dimensions={0} | all-to-all | bytes 2097152 | tf_op jit(solution)/shard_map/all_to_all | solution.py:51
  117.8 0.9 reduce_sum.52
  118.8 16.8 %all-to-all-start.3 = ((bf16[32,32,128]{2,1,0:T(8,128)(2,1)}), bf16[32,32,128]{2,1,0:T(8,128)(2,1)S(1)}, u32[]{:S(2)}, u32[]{:S(2)}) async-start(bf16[32,32,128]{2,1,0:T(8,128)(2,1)} %bitcast.15), calls=%async_computation.3 | async-start | bytes 524288 | tf_op jit(solution)/shard_map/all_to_all | solution.py:248
  135.6 22.2 %all-to-all-done.3 = bf16[32,32,128]{2,1,0:T(8,128)(2,1)S(1)} async-done(((bf16[32,32,128]{2,1,0:T(8,128)(2,1)}), bf16[32,32,128]{2,1,0:T(8,128)(2,1)S(1)}, u32[]{:S(2)}, u32[]{:S(2)}) %all-to-all-start.3) | async-done | bytes 262176 | tf_op jit(solution)/shard_map/all_to_all | solution.py:248
  157.8 0.9 fusion
  158.7 0.2 broadcast_in_dim.58
  158.9 19.6 %all_to_all.28.columns_ref = bf16[16,256,128]{2,1,0:T(8,128)(2,1)} all-to-all(bf16[16,256,128]{2,1,0:T(8,128)(2,1)S(1)} %broadcast_in_dim.58), channel_id=1, replica_groups=mesh['z'=16,'c'=2,'y'=4,'x'=4] {'y','x'}, dimensions={0} | all-to-all | bytes 2097152 | tf_op jit(solution)/shard_map/all_to_all | solution.py:259
  178.5 3.4 %assemble.1 = bf16[256,2048]{1,0:T(8,128)(2,1)} custom-call(bf16[16,256,128]{2,1,0:T(8,128)(2,1)} %all_to_all.28.columns_ref), custom_call_target="tpu_custom_call" | custom-call | tf_op jit(solution)/shard_map/assemble/pallas_call | solution.py:153
  (12 shorter events, 0.1 us)
Async XLA Ops:
  0.0 25.0 %copy-start = (bf16[512,128]{1,0:T(8,128)(2,1)S(1)}, bf16[512,128]{1,0:T(8,128)(2,1)}, u32[]{:S(2)}) copy-start(bf16[512,128]{1,0:T(8,128)(2,1)} %param.14) | copy-start | bytes 393220
  2.1 20.1 %copy-start.3 = (s32[256,2]{0,1:T(2,128)S(1)}, s32[256,2]{0,1:T(2,128)}, u32[]{:S(2)}) copy-start(s32[256,2]{0,1:T(2,128)} %param.17) | copy-start | bytes 6148
  2.1 22.0 %copy-start.7 = (bf16[256,256]{1,0:T(8,128)(2,1)S(1)}, bf16[256,256]{1,0:T(8,128)(2,1)}, u32[]{:S(2)}) copy-start(bf16[256,256]{1,0:T(8,128)(2,1)} %constant.70.clone) | copy-start | bytes 393220
  2.1 86.5 %collective-permute-start.2 = (bf16[672,2048]{1,0:T(8,128)(2,1)S(1)}, bf16[672,2048]{1,0:T(8,128)(2,1)}, u32[]{:S(2)}, u32[]{:S(2)}) collective-permute-start(bf16[672,2048]{1,0:T(8,128)(2,1)S(1)} %pad_maximum_fusion.refs_0_), channel_id=1, source_target_pairs={{0,1},{1,2},{2,3},{3,0},{4,5},{5,6},{6,7},{7,4},{8,9},{9,10},{10,1... | collective-permute-start | bytes 8257544 | tf_op jit(solution)/shard_map/ppermute | solution.py:46
  6.3 82.3 %collective-permute-start.3 = (bf16[672,2048]{1,0:T(8,128)(2,1)S(1)}, bf16[672,2048]{1,0:T(8,128)(2,1)}, u32[]{:S(2)}, u32[]{:S(2)}) collective-permute-start(bf16[672,2048]{1,0:T(8,128)(2,1)S(1)} %pad_maximum_fusion.refs_0_), channel_id=1, source_target_pairs={{0,3},{1,0},{2,1},{3,2},{4,7},{5,4},{6,5},{7,6},{8,11},{9,8},{10,9... | collective-permute-start | bytes 8257544 | tf_op jit(solution)/shard_map/ppermute | solution.py:46
  9.7 85.4 %collective-permute-start.1 = (bf16[672,2048]{1,0:T(8,128)(2,1)S(1)}, bf16[672,2048]{1,0:T(8,128)(2,1)}, u32[]{:S(2)}, u32[]{:S(2)}) collective-permute-start(bf16[672,2048]{1,0:T(8,128)(2,1)S(1)} %pad_maximum_fusion.refs_0_), channel_id=1, source_target_pairs={{0,2},{1,3},{2,0},{3,1},{4,6},{5,7},{6,4},{7,5},{8,10},{9,11},{10,... | collective-permute-start | bytes 8257544 | tf_op jit(solution)/shard_map/ppermute | solution.py:46
  14.1 10.3 %collective-permute-start = (bf16[16,2048]{1,0:T(8,128)(2,1)S(1)}, bf16[16,2048]{1,0:T(8,128)(2,1)S(1)}, u32[]{:S(2)}, u32[]{:S(2)}) collective-permute-start(bf16[16,2048]{1,0:T(8,128)(2,1)S(1)} %slice.53), channel_id=1, source_target_pairs={{0,16},{16,32},{32,48},{48,64},{64,80},{80,96},{96,112},{112,128},... | collective-permute-start | bytes 196616 | tf_op jit(solution)/shard_map/ppermute | solution.py:29
  18.9 3.0 %copy-start.2 = (bf16[256,2048]{1,0:T(8,128)(2,1)S(1)}, bf16[256,2048]{1,0:T(8,128)(2,1)}, u32[]{:S(2)}) copy-start(bf16[256,2048]{1,0:T(8,128)(2,1)} %param.12) | copy-start | bytes 3145732
  18.9 5.5 %copy-start.5 = (s32[256]{0:T(256)S(1)}, s32[256]{0:T(256)}, u32[]{:S(2)}) copy-start(s32[256]{0:T(256)} %constant.71.clone) | copy-start | bytes 3076
  24.7 0.7 copy-start.6
  88.6 1.2 copy-start.1
  98.0 37.6 %copy-start.4 = (f32[256,2]{0,1:T(2,128)S(1)}, f32[256,2]{0,1:T(2,128)}, u32[]{:S(2)}) copy-start(f32[256,2]{0,1:T(2,128)} %param.18) | copy-start | bytes 6148
  118.8 39.1 %all-to-all-start.3 = ((bf16[32,32,128]{2,1,0:T(8,128)(2,1)}), bf16[32,32,128]{2,1,0:T(8,128)(2,1)S(1)}, u32[]{:S(2)}, u32[]{:S(2)}) async-start(bf16[32,32,128]{2,1,0:T(8,128)(2,1)} %bitcast.15), calls=%async_computation.3 | async-start | bytes 524288 | tf_op jit(solution)/shard_map/all_to_all | solution.py:248

commit v4 on v3

--- a/solution.py
+++ b/solution.py
@@ -55,7 +55,16 @@
     return jnp.where(swapped == 0, t, (t % side) * side + t // side)
 
 
-def norm_kernel(side, core_ref, x_ref, gain_ref, normed_ref):
+def expert_kernel(side, core_ref, x_ref, gain_ref, *refs):
+    pieces = (len(refs) - 3) // 2
+    sources, out_ref, normed_ref = (refs[:pieces], refs[pieces], refs[pieces + 1])
+    weights, semaphores = (refs[pieces + 2 : 2 * pieces + 2], refs[-1])
+    copies = [
+        pltpu.make_async_copy(source, target, semaphores.at[i])
+        for i, (source, target) in enumerate(zip(sources, weights))
+    ]
+    for copy in copies:
+        copy.start()
     count, rows, lanes = x_ref.shape
     squares = jnp.zeros((rows, lanes), jnp.float32)
     for t in range(count):
@@ -66,86 +75,71 @@
         columns = slice(t * lanes, (t + 1) * lanes)
         values = x_ref[place(t, side, core_ref[0])].astype(jnp.float32)
         normed_ref[:, columns] = (values * inverse * gain_ref[:, columns]).astype(jnp.bfloat16)
-
-
-def expert_kernel(side, parts, core_ref, normed_ref, *refs):
-    weight_refs, refs = (refs[:parts], refs[parts:])
-    last = len(refs[-1].shape) == 3
-    total_refs, out_ref = (refs[:-1], refs[-1])
-    width = normed_ref.shape[1]
-    units = weight_refs[0].shape[0] // 3
+    units = weights[0].shape[0] // 3
     contract = (((1,), (1,)), ((), ()))
     normed = normed_ref[...]
-    hidden = []
-    for ref in weight_refs:
-        gate = lax.dot_general(normed, ref[:units], contract, preferred_element_type=jnp.float32)
-        up = lax.dot_general(
-            normed, ref[units : 2 * units], contract, preferred_element_type=jnp.float32
-        )
+    hidden, downs = ([], [])
+    for i in range(pieces - 1):
+        copies[i].wait()
+        gate_rows, up_rows = (weights[i][:units], None)
+        if i < pieces - 2:
+            up_rows = weights[i][units : 2 * units]
+            downs.append(weights[i].at[2 * units :])
+        else:
+            copies[i + 1].wait()
+            cut = weights[i].shape[0]
+            up_rows = jnp.concatenate(
+                [weights[i][units:], weights[i + 1][: 2 * units - cut]], axis=0
+            )
+            downs.append(weights[i + 1].at[2 * units - cut :])
+        gate = lax.dot_general(normed, gate_rows, contract, preferred_element_type=jnp.float32)
+        up = lax.dot_general(normed, up_rows, contract, preferred_element_type=jnp.float32)
         hidden.append((gate * (1.0 / (1.0 + jnp.exp(-gate))) * up).astype(jnp.bfloat16))
-    step = 2 * LANES
-    for first in range(0, width, step):
-        columns = slice(first, first + step)
+    for t in range(0, count, 2):
         total = 0.0
-        for part, ref in zip(hidden, weight_refs):
+        for part, down in zip(hidden, downs):
             total = total + jnp.dot(
-                part, ref[2 * units :, columns], preferred_element_type=jnp.float32
+                part,
+                down[:, t * lanes : (t + 2) * lanes],
+                preferred_element_type=jnp.float32,
             )
-        for ref in total_refs:
-            total = total + ref[:, columns]
-        if last:
-            for half in range(2):
-                t = first // LANES + half
-                out_ref[place(t, side, core_ref[0])] = total[
-                    :, half * LANES : (half + 1) * LANES
-                ].astype(jnp.bfloat16)
-        else:
-            out_ref[:, columns] = total
+        total = total.astype(jnp.bfloat16)
+        out_ref[place(t, side, core_ref[0])] = total[:, :lanes]
+        out_ref[place(t + 1, side, core_ref[0])] = total[:, lanes:]
 
 
 SCALARS = pl.BlockSpec(memory_space=pltpu.SMEM)
 VECTORS = pl.BlockSpec(memory_space=pltpu.VMEM)
-
-
-def norm_rows(blocks, core, gain, side):
+ANYWHERE = pl.BlockSpec(memory_space=pl.ANY)
+
+
+def expert(blocks, core, gain, weights, side):
     count, rows, lanes = blocks.shape
+    width = count * lanes
+    units = weights[0].shape[0] // 3
     return pl.pallas_call(
-        functools.partial(norm_kernel, side),
-        out_shape=jax.ShapeDtypeStruct((rows, count * lanes), jnp.bfloat16),
-        in_specs=[SCALARS, VECTORS, VECTORS],
+        functools.partial(expert_kernel, side),
+        out_shape=jax.ShapeDtypeStruct(blocks.shape, jnp.bfloat16),
+        in_specs=[SCALARS, VECTORS, VECTORS] + [ANYWHERE] * len(weights),
         out_specs=VECTORS,
+        scratch_shapes=[pltpu.VMEM((rows, width), jnp.bfloat16)]
+        + [pltpu.VMEM(w.shape, w.dtype) for w in weights]
+        + [pltpu.SemaphoreType.DMA((len(weights),))],
+        compiler_params=pltpu.CompilerParams(vmem_limit_bytes=32 * 2**20),
         cost_estimate=pl.CostEstimate(
-            flops=4 * blocks.size, bytes_accessed=4 * blocks.size, transcendentals=rows
-        ),
-        name="norm",
-    )(core, blocks, gain[None])
-
-
-def expert(normed, core, weights, totals, side, last):
-    rows, width = normed.shape
-    units = weights[0].shape[0] // 3
-    if last:
-        out = jax.ShapeDtypeStruct((width // LANES, rows, LANES), jnp.bfloat16)
-    else:
-        out = jax.ShapeDtypeStruct((rows, width), jnp.float32)
-    return pl.pallas_call(
-        functools.partial(expert_kernel, side, len(weights)),
-        out_shape=out,
-        in_specs=[SCALARS] + [VECTORS] * (1 + len(weights) + len(totals)),
-        out_specs=VECTORS,
-        compiler_params=pltpu.CompilerParams(vmem_limit_bytes=40 * 2**20),
-        cost_estimate=pl.CostEstimate(
-            flops=6 * rows * units * width * len(weights),
-            bytes_accessed=6 * units * width * len(weights),
-            transcendentals=rows * units * len(weights),
+            flops=6 * rows * units * width * side,
+            bytes_accessed=6 * units * width * side,
+            transcendentals=rows * units * side,
         ),
         name="expert",
-    )(core, normed, *weights, *totals)
+    )(core, blocks, gain[None], *weights)
 
 
 def assemble_kernel(columns_ref, out_ref):
+    rows = out_ref.shape[0]
+    here = pl.ds(pl.multiple_of(pl.program_id(0) * rows, rows), rows)
     for t in range(columns_ref.shape[0]):
-        out_ref[:, t * LANES : (t + 1) * LANES] = columns_ref[t]
+        out_ref[:, t * LANES : (t + 1) * LANES] = columns_ref[t, here]
 
 
 def assemble(columns, rows=64):
@@ -154,13 +148,13 @@
         assemble_kernel,
         out_shape=jax.ShapeDtypeStruct((total, count * lanes), columns.dtype),
         grid=(total // rows,),
-        in_specs=[pl.BlockSpec((count, rows, lanes), lambda i: (0, i, 0))],
+        in_specs=[VECTORS],
         out_specs=pl.BlockSpec((rows, count * lanes), lambda i: (i, 0)),
         name="assemble",
     )(columns)
 
 
-def shards(
+def layer(
     residual_in,
     mix_gain,
     pool_weight,
@@ -183,7 +177,8 @@
     group_index = tp_index * col_count // group_width
 
     own = jnp.concatenate([gate_weight[0].T, up_weight[0].T, down_weight[0]], axis=0)
-    others = [from_quad(own, steps) for steps in (1, -1, 2)]
+    left = from_quad(own, 1)
+    right = from_quad(own, -1)
     rim = from_behind(residual_in[tok_count - SPAN :], SP, 1)
 
     def normed_group(rows):
@@ -232,7 +227,13 @@
         (((0,), (0,)), ((), ())),
         preferred_element_type=jnp.float32,
     ).astype(jnp.bfloat16)
-    arrived = lax.all_to_all(outgoing.reshape(sp_count, slots, col_count), SP, 0, 0, tiled=True)
+    outgoing = outgoing.reshape(sp_count, slots, col_count)
+    arrived = lax.all_to_all(outgoing, SP, 0, 0, tiled=True)
+    half = own.shape[0] // 2
+    upper = left[:half]
+    lower = right[half:]
+    upper = from_quad(upper, 1)
+    lower = from_quad(lower, -1)
     arrived = arrived.reshape(sp_count * slots, col_count)
 
     side = lax.axis_size("x")
@@ -240,9 +241,7 @@
     quarter = arrived.reshape(1, side, -1, col_count)
     quarter = jnp.broadcast_to(quarter, (side, *quarter.shape[1:]))
     gathered = exchange(quarter.reshape(tp_count, -1, col_count))
-    normed = norm_rows(gathered, core, ffn_gain, side)
-    total = expert(normed, core, [own, *others[:2]], [], side, False)
-    term = expert(normed, core, others[2:], [total], side, True)
+    term = expert(gathered, core, ffn_gain, [own, left, right, upper, lower], side)
     summed = exchange(term).reshape(quarter.shape)
     expert_out = jnp.sum(summed.astype(jnp.float32), axis=0).astype(jnp.bfloat16)
     returned = lax.all_to_all(
@@ -263,7 +262,7 @@
 def solution(mesh):
     torus = Mesh(mesh.devices.reshape(-1, 2, 4, mesh.shape["tp"] // 4), ALL)
     return jax.shard_map(
-        shards,
+        layer,
         mesh=torus,
         in_specs=(
             P(SP, None),

time: 183 us -> 170 us (0.929)
  blocking collectives: 97.9 us -> 56.8 us
  starting transfers between devices: 32.6 us -> 51.4 us
  waiting for transfers between devices: 22.2 us -> 32.5 us
  Pallas kernels: 14.3 us -> 8.48 us
  local copies, waits for them, and re-layouts: 3.75 us -> 7.79 us
    all_to_all x2 -> x1, blocking collectives: 56.2 us -> 19.6 us  [layer(): columns = lax.all_to_all(copies, TP, 0, 0, tiled=True)]
    all_to_all x1 -> x2, starting transfers between devices: 16.8 us -> 32.6 us  [the longest x1 18.2 us: layer(): lax.all_to_all(expert_out.reshape(sp_count, slots, col_count), SP, 0, 0,...]
    all_to_all x1 -> x2, waiting for transfers between devices: 22.2 us -> 32.5 us  [the longest x1 22.2 us: layer(): lax.all_to_all(expert_out.reshape(sp_count, slots, col_count), SP, 0, 0,...]
    slice x4 -> x6, local copies, waits for them, and re-layouts: 0.98 us -> 6.24 us  [the longest x1 2.67 us: layer(): upper = left[:half]]
    pallas_call x3 -> x1, Pallas kernels: 10.8 us -> 5.67 us  [expert(): pl.pallas_call(functools.partial(expert_kernel, side), out_shape=jax.Shap...]
    all_to_all x2, blocking collectives: 41.8 us -> 37.2 us  [exchange(): lax.all_to_all(blocks, ALL, 0, 0, tiled=True, axis_index_groups=groups)]
    ppermute x3 -> x4, starting transfers between devices: 11.1 us -> 14.2 us  [from_quad(): return lax.ppermute(value, ALL, pairs)]
  transfers between devices with their start and end apart: 5 -> 7, of which waited for: 1 -> 2; matrix products, arithmetic and copies ran while one was open for 5% -> 9% of each run, Pallas kernels for 4% -> 0%
where the time goes in v4:
time: 170 us; the launch traced here: 169 us
  blocking collectives  56.8 us (33%)
  starting transfers between devices  51.4 us (30%)
  waiting for transfers between devices  32.5 us (19%)
  Pallas kernels  8.48 us (5%)
  other arithmetic  7.84 us (5%)
  local copies, waits for them, and re-layouts  7.79 us (5%)
  matrix products  3.63 us (2%)
    all_to_all x2, blocking collectives, exchange(): lax.all_to_all(blocks, ALL, 0, 0, tiled=True, axis_index_groups=groups)  37.2 us
    all_to_all x1, waiting for transfers between devices, layer(): lax.all_to_all(expert_out.reshape(sp_count, slots, col_count), SP, 0, 0,...  22.2 us
    all_to_all x1, blocking collectives, layer(): columns = lax.all_to_all(copies, TP, 0, 0, tiled=True)  19.6 us
    all_to_all x1, starting transfers between devices, layer(): lax.all_to_all(expert_out.reshape(sp_count, slots, col_count), SP, 0, 0,...  18.2 us
    all_to_all x1, starting transfers between devices, layer(): arrived = lax.all_to_all(outgoing, SP, 0, 0, tiled=True)  14.5 us
    ppermute x4, starting transfers between devices, from_quad(): return lax.ppermute(value, ALL, pairs)  14.2 us
    all_to_all x1, waiting for transfers between devices, layer(): arrived = lax.all_to_all(outgoing, SP, 0, 0, tiled=True)  10.3 us
    pallas_call x1, Pallas kernels, expert(): pl.pallas_call(functools.partial(expert_kernel, side), out_shape=jax.Shap...  5.67 us
  transfers between devices with their start and end apart: 7, of which 2 were waited for; matrix products, arithmetic and copies ran while one was open for 9% of the time, Pallas kernels for 0%

profile of v4, /device:TPU:1, one launch (start us, length us, event | category | flops | bytes accessed | tf_op | source)
XLA Modules:
  0.0 168.8 jit_solution(15811223574761779786)
XLA Ops:
  0.0 0.0 copy-start
  0.0 2.1 %pad_maximum_fusion.refs_0_ = bf16[672,2048]{1,0:T(8,128)(2,1)S(1)} fusion(bf16[224,2048]{1,0:T(8,128)(2,1)} %bitcast.27, bf16[224,2048]{1,0:T(8,128)(2,1)} %bitcast.28, bf16[224,2048]{1,0:T(8,128)(2,1)} %bitcast.29), kind=kLoop, calls=%fused_computation | loop fusion | flops 8257536 | bytes 5505024 | tf_op jit(solution)/shard_map/concatenate | solution.py:179
  2.1 0.0 copy-start.3
  2.1 0.0 copy-start.7
  2.1 4.2 %collective-permute-start.1 = (bf16[672,2048]{1,0:T(8,128)(2,1)S(1)}, bf16[672,2048]{1,0:T(8,128)(2,1)}, u32[]{:S(2)}, u32[]{:S(2)}) collective-permute-start(bf16[672,2048]{1,0:T(8,128)(2,1)S(1)} %pad_maximum_fusion.refs_0_), channel_id=1, source_target_pairs={{0,1},{1,2},{2,3},{3,0},{4,5},{5,6},{6,7},{7,4},{8,9},{9,10},{10,1... | collective-permute-start | bytes 8257544 | tf_op jit(solution)/shard_map/ppermute | solution.py:46
  6.3 3.4 %collective-permute-start.2 = (bf16[672,2048]{1,0:T(8,128)(2,1)S(1)}, bf16[672,2048]{1,0:T(8,128)(2,1)}, u32[]{:S(2)}, u32[]{:S(2)}) collective-permute-start(bf16[672,2048]{1,0:T(8,128)(2,1)S(1)} %pad_maximum_fusion.refs_0_), channel_id=1, source_target_pairs={{0,3},{1,0},{2,1},{3,2},{4,7},{5,4},{6,5},{7,6},{8,11},{9,8},{10,9... | collective-permute-start | bytes 8257544 | tf_op jit(solution)/shard_map/ppermute | solution.py:46
  9.7 0.8 slice.59
  10.5 4.6 %collective-permute-start = (bf16[16,2048]{1,0:T(8,128)(2,1)S(1)}, bf16[16,2048]{1,0:T(8,128)(2,1)S(1)}, u32[]{:S(2)}, u32[]{:S(2)}) collective-permute-start(bf16[16,2048]{1,0:T(8,128)(2,1)S(1)} %slice.59), channel_id=1, source_target_pairs={{0,16},{16,32},{32,48},{48,64},{64,80},{80,96},{96,112},{112,128},... | collective-permute-start | bytes 196616 | tf_op jit(solution)/shard_map/ppermute | solution.py:29
  15.1 0.0 copy-start.2
  15.1 0.0 copy-start.5
  15.1 2.9 %convert_element_type.58 = f32[256,2048]{1,0:T(8,128)} convert(bf16[256,2048]{1,0:T(8,128)(2,1)} %param.12) | non-fusion elementwise | flops 524288 | bytes 3145728 | tf_op jit(solution)/shard_map/convert_element_type | solution.py:185
  18.0 0.3 multiply_reduce_fusion
  18.4 0.8 dynamic_slice.15
  19.2 1.2 multiply_reduce-precision_fusion
  20.4 0.2 select_reduce_fusion.1
  20.6 0.0 collective-permute-done
  20.6 0.1 multiply_reduce_fusion.1
  20.8 0.1 multiply_reduce-precision_fusion.1
  20.9 0.1 fusion.10
  20.9 0.0 copy-start.6
  21.0 0.1 slice_add_fusion.1
  21.0 0.1 slice_add_fusion
  21.1 0.1 fusion.26
  21.2 0.4 copy-done.6
  21.6 1.3 fusion.4
  22.9 1.3 convolution_convert_fusion
  24.2 14.5 %all-to-all-start = ((bf16[32,32,128]{2,1,0:T(8,128)(2,1)}), bf16[32,32,128]{2,1,0:T(8,128)(2,1)S(1)}, u32[]{:S(2)}, u32[]{:S(2)}) async-start(bf16[32,32,128]{2,1,0:T(8,128)(2,1)} %bitcast.5), calls=%async_computation | async-start | bytes 524288 | tf_op jit(solution)/shard_map/all_to_all | solution.py:231
  38.6 0.0 collective-permute-done.1.refs_1_
  38.6 2.7 %slice.91 = bf16[336,2048]{1,0:T(8,128)(2,1)} slice(bf16[672,2048]{1,0:T(8,128)(2,1)} %collective-permute-done.1.refs_1_), slice={[0:336], [0:2048]} | slice | bytes 2752512 | tf_op jit(solution)/shard_map/slice | solution.py:233
  41.3 3.3 %collective-permute-start.3 = (bf16[336,2048]{1,0:T(8,128)(2,1)}, bf16[336,2048]{1,0:T(8,128)(2,1)}, u32[]{:S(2)}, u32[]{:S(2)}) collective-permute-start(bf16[336,2048]{1,0:T(8,128)(2,1)} %slice.91), channel_id=1, source_target_pairs={{0,1},{1,2},{2,3},{3,0},{4,5},{5,6},{6,7},{7,4},{8,9},{9,10},{10,1... | collective-permute-start | bytes 4128776 | tf_op jit(solution)/shard_map/ppermute | solution.py:46
  44.7 0.0 collective-permute-done.2.refs_2_
  44.7 2.6 %slice.92 = bf16[336,2048]{1,0:T(8,128)(2,1)} slice(bf16[672,2048]{1,0:T(8,128)(2,1)} %collective-permute-done.2.refs_2_), slice={[336:672], [0:2048]} | slice | bytes 2752512 | tf_op jit(solution)/shard_map/slice | solution.py:234
  47.3 3.3 %collective-permute-start.4 = (bf16[336,2048]{1,0:T(8,128)(2,1)}, bf16[336,2048]{1,0:T(8,128)(2,1)}, u32[]{:S(2)}, u32[]{:S(2)}) collective-permute-start(bf16[336,2048]{1,0:T(8,128)(2,1)} %slice.92), channel_id=1, source_target_pairs={{0,3},{1,0},{2,1},{3,2},{4,7},{5,4},{6,5},{7,6},{8,11},{9,8},{10,9... | collective-permute-start | bytes 4128776 | tf_op jit(solution)/shard_map/ppermute | solution.py:46
  50.6 10.3 %all-to-all-done = bf16[32,32,128]{2,1,0:T(8,128)(2,1)S(1)} async-done(((bf16[32,32,128]{2,1,0:T(8,128)(2,1)}), bf16[32,32,128]{2,1,0:T(8,128)(2,1)S(1)}, u32[]{:S(2)}, u32[]{:S(2)}) %all-to-all-start) | async-done | bytes 262176 | tf_op jit(solution)/shard_map/all_to_all | solution.py:231
  60.9 0.2 broadcast_in_dim.56
  61.1 21.9 %all_to_all.25.x_ref = bf16[16,256,128]{2,1,0:T(8,128)(2,1)S(1)} all-to-all(bf16[16,256,128]{2,1,0:T(8,128)(2,1)S(1)} %bitcast.24), channel_id=1, replica_groups={{0,1,2,3,4,5,6,7,8,9,10,11,12,13,14,15},{16,20,24,28,17,21,25,29,18,22,..., dimensions={0} | all-to-all | bytes 2097152 | tf_op jit(solution)/shard_map/all_to_all | solution.py:51
  83.0 0.0 collective-permute-done.3.refs_3_
  83.0 0.0 collective-permute-done.4.refs_4_
  83.0 5.7 %expert.1 = bf16[16,256,128]{2,1,0:T(8,128)(2,1)S(1)} custom-call(s32[1]{0:T(128)} %bitcast.4.core_ref, bf16[16,256,128]{2,1,0:T(8,128)(2,1)S(1)} %all_to_all.25.x_ref, f32[1,2048]{1,0:T(1,128)S(1)} %bitcast.23, bf16[672,2048]{1,0:T(8,128)(2,1)S(1)} %pad_maximum_fusion.refs_0_, bf16[672,2048]{1,0:T(8,128)(2,1)} %collective-permute-done.1.refs_1_, ...), custom_call_target="tpu_custom_call" | custom-call | flops 2818572288 | bytes 11010048 | tf_op jit(solution)/shard_map/expert/pallas_call | solution.py:120
  88.7 0.0 copy-start.4
  88.7 15.2 %all_to_all.26 = bf16[16,256,128]{2,1,0:T(8,128)(2,1)S(1)} all-to-all(bf16[16,256,128]{2,1,0:T(8,128)(2,1)S(1)} %expert.1), channel_id=1, replica_groups={{0,1,2,3,4,5,6,7,8,9,10,11,12,13,14,15},{16,20,24,28,17,21,25,29,18,22,..., dimensions={0} | all-to-all | bytes 2097152 | tf_op jit(solution)/shard_map/all_to_all | solution.py:51
  104.0 0.9 reduce_sum.52
  104.9 18.2 %all-to-all-start.3 = ((bf16[32,32,128]{2,1,0:T(8,128)(2,1)}), bf16[32,32,128]{2,1,0:T(8,128)(2,1)S(1)}, u32[]{:S(2)}, u32[]{:S(2)}) async-start(bf16[32,32,128]{2,1,0:T(8,128)(2,1)} %bitcast.15), calls=%async_computation.3 | async-start | bytes 524288 | tf_op jit(solution)/shard_map/all_to_all | solution.py:247
  123.1 22.2 %all-to-all-done.3 = bf16[32,32,128]{2,1,0:T(8,128)(2,1)S(1)} async-done(((bf16[32,32,128]{2,1,0:T(8,128)(2,1)}), bf16[32,32,128]{2,1,0:T(8,128)(2,1)S(1)}, u32[]{:S(2)}, u32[]{:S(2)}) %all-to-all-start.3) | async-done | bytes 262176 | tf_op jit(solution)/shard_map/all_to_all | solution.py:247
  145.3 0.9 fusion
  146.2 0.2 broadcast_in_dim.58
  146.4 19.6 %all_to_all.27.columns_ref = bf16[16,256,128]{2,1,0:T(8,128)(2,1)} all-to-all(bf16[16,256,128]{2,1,0:T(8,128)(2,1)S(1)} %broadcast_in_dim.58), channel_id=1, replica_groups=mesh['z'=16,'c'=2,'y'=4,'x'=4] {'y','x'}, dimensions={0} | all-to-all | bytes 2097152 | tf_op jit(solution)/shard_map/all_to_all | solution.py:258
  166.0 2.8 %assemble.1 = bf16[256,2048]{1,0:T(8,128)(2,1)} custom-call(bf16[16,256,128]{2,1,0:T(8,128)(2,1)} %all_to_all.27.columns_ref), custom_call_target="tpu_custom_call" | custom-call | tf_op jit(solution)/shard_map/assemble/pallas_call | solution.py:147
  (15 shorter events, 0.1 us)
Async XLA Ops:
  0.0 21.2 %copy-start = (bf16[512,128]{1,0:T(8,128)(2,1)S(1)}, bf16[512,128]{1,0:T(8,128)(2,1)}, u32[]{:S(2)}) copy-start(bf16[512,128]{1,0:T(8,128)(2,1)} %param.14) | copy-start | bytes 393220
  2.1 16.3 %copy-start.3 = (s32[256,2]{0,1:T(2,128)S(1)}, s32[256,2]{0,1:T(2,128)}, u32[]{:S(2)}) copy-start(s32[256,2]{0,1:T(2,128)} %param.17) | copy-start | bytes 6148
  2.1 18.2 %copy-start.7 = (bf16[256,256]{1,0:T(8,128)(2,1)S(1)}, bf16[256,256]{1,0:T(8,128)(2,1)}, u32[]{:S(2)}) copy-start(bf16[256,256]{1,0:T(8,128)(2,1)} %constant.70.clone) | copy-start | bytes 393220
  2.1 36.5 %collective-permute-start.1 = (bf16[672,2048]{1,0:T(8,128)(2,1)S(1)}, bf16[672,2048]{1,0:T(8,128)(2,1)}, u32[]{:S(2)}, u32[]{:S(2)}) collective-permute-start(bf16[672,2048]{1,0:T(8,128)(2,1)S(1)} %pad_maximum_fusion.refs_0_), channel_id=1, source_target_pairs={{0,1},{1,2},{2,3},{3,0},{4,5},{5,6},{6,7},{7,4},{8,9},{9,10},{10,1... | collective-permute-start | bytes 8257544 | tf_op jit(solution)/shard_map/ppermute | solution.py:46
  6.3 38.4 %collective-permute-start.2 = (bf16[672,2048]{1,0:T(8,128)(2,1)S(1)}, bf16[672,2048]{1,0:T(8,128)(2,1)}, u32[]{:S(2)}, u32[]{:S(2)}) collective-permute-start(bf16[672,2048]{1,0:T(8,128)(2,1)S(1)} %pad_maximum_fusion.refs_0_), channel_id=1, source_target_pairs={{0,3},{1,0},{2,1},{3,2},{4,7},{5,4},{6,5},{7,6},{8,11},{9,8},{10,9... | collective-permute-start | bytes 8257544 | tf_op jit(solution)/shard_map/ppermute | solution.py:46
  10.5 10.1 %collective-permute-start = (bf16[16,2048]{1,0:T(8,128)(2,1)S(1)}, bf16[16,2048]{1,0:T(8,128)(2,1)S(1)}, u32[]{:S(2)}, u32[]{:S(2)}) collective-permute-start(bf16[16,2048]{1,0:T(8,128)(2,1)S(1)} %slice.59), channel_id=1, source_target_pairs={{0,16},{16,32},{32,48},{48,64},{64,80},{80,96},{96,112},{112,128},... | collective-permute-start | bytes 196616 | tf_op jit(solution)/shard_map/ppermute | solution.py:29
  15.1 2.9 %copy-start.2 = (bf16[256,2048]{1,0:T(8,128)(2,1)S(1)}, bf16[256,2048]{1,0:T(8,128)(2,1)}, u32[]{:S(2)}) copy-start(bf16[256,2048]{1,0:T(8,128)(2,1)} %param.12) | copy-start | bytes 3145732
  15.1 5.4 %copy-start.5 = (s32[256]{0:T(256)S(1)}, s32[256]{0:T(256)}, u32[]{:S(2)}) copy-start(s32[256]{0:T(256)} %constant.71.clone) | copy-start | bytes 3076
  20.9 0.7 copy-start.6
  24.2 36.7 %all-to-all-start = ((bf16[32,32,128]{2,1,0:T(8,128)(2,1)}), bf16[32,32,128]{2,1,0:T(8,128)(2,1)S(1)}, u32[]{:S(2)}, u32[]{:S(2)}) async-start(bf16[32,32,128]{2,1,0:T(8,128)(2,1)} %bitcast.5), calls=%async_computation | async-start | bytes 524288 | tf_op jit(solution)/shard_map/all_to_all | solution.py:231
  41.3 41.7 %copy-start.1 = (f32[2048]{0:T(1024)S(1)}, f32[2048]{0:T(1024)}, u32[]{:S(2)}) copy-start(f32[2048]{0:T(1024)} %param.16) | copy-start | bytes 24580
  41.3 41.7 %collective-permute-start.3 = (bf16[336,2048]{1,0:T(8,128)(2,1)}, bf16[336,2048]{1,0:T(8,128)(2,1)}, u32[]{:S(2)}, u32[]{:S(2)}) collective-permute-start(bf16[336,2048]{1,0:T(8,128)(2,1)} %slice.91), channel_id=1, source_target_pairs={{0,1},{1,2},{2,3},{3,0},{4,5},{5,6},{6,7},{7,4},{8,9},{9,10},{10,1... | collective-permute-start | bytes 4128776 | tf_op jit(solution)/shard_map/ppermute | solution.py:46
  47.3 35.8 %collective-permute-start.4 = (bf16[336,2048]{1,0:T(8,128)(2,1)}, bf16[336,2048]{1,0:T(8,128)(2,1)}, u32[]{:S(2)}, u32[]{:S(2)}) collective-permute-start(bf16[336,2048]{1,0:T(8,128)(2,1)} %slice.92), channel_id=1, source_target_pairs={{0,3},{1,0},{2,1},{3,2},{4,7},{5,4},{6,5},{7,6},{8,11},{9,8},{10,9... | collective-permute-start | bytes 4128776 | tf_op jit(solution)/shard_map/ppermute | solution.py:46
  88.7 34.4 %copy-start.4 = (f32[256,2]{0,1:T(2,128)S(1)}, f32[256,2]{0,1:T(2,128)}, u32[]{:S(2)}) copy-start(f32[256,2]{0,1:T(2,128)} %param.18) | copy-start | bytes 6148
  104.9 40.5 %all-to-all-start.3 = ((bf16[32,32,128]{2,1,0:T(8,128)(2,1)}), bf16[32,32,128]{2,1,0:T(8,128)(2,1)S(1)}, u32[]{:S(2)}, u32[]{:S(2)}) async-start(bf16[32,32,128]{2,1,0:T(8,128)(2,1)} %bitcast.15), calls=%async_computation.3 | async-start | bytes 524288 | tf_op jit(solution)/shard_map/all_to_all | solution.py:247

commit v5 on v4

--- a/solution.py
+++ b/solution.py
@@ -135,21 +135,174 @@
     )(core, blocks, gain[None], *weights)
 
 
-def assemble_kernel(columns_ref, out_ref):
-    rows = out_ref.shape[0]
-    here = pl.ds(pl.multiple_of(pl.program_id(0) * rows, rows), rows)
+def inverse_rms(ref):
+    rows, width = ref.shape
+    squares = jnp.zeros((rows, LANES), jnp.float32)
+    for first in range(0, width, LANES):
+        values = ref[:, first : first + LANES].astype(jnp.float32)
+        squares = squares + values * values
+    return lax.rsqrt(jnp.sum(squares, axis=1, keepdims=True) / width + EPS)
+
+
+def mixer_kernel(
+    experts,
+    index_ref,
+    ids_ref,
+    x_ref,
+    rim_ref,
+    gain_ref,
+    weight_ref,
+    scale_ref,
+    outgoing_ref,
+    after_ref,
+    target_ref,
+):
+    group, tp_index, sp_index = (index_ref[0], index_ref[1], index_ref[2])
+    rows = x_ref.shape[0]
+    span = rim_ref.shape[0]
+    group_width, col_count = weight_ref.shape
+    columns = pl.ds(pl.multiple_of(group * group_width, group_width), group_width)
+    gain = gain_ref[:, columns]
+
+    def normed(ref):
+        return (ref[:, columns].astype(jnp.float32) * inverse_rms(ref) * gain).astype(jnp.bfloat16)
+
+    window = jnp.left_shift(2, group)
+    here = normed(x_ref)
+    row = lax.broadcasted_iota(jnp.int32, (rows, rows), 0)
+    col = lax.broadcasted_iota(jnp.int32, (rows, rows), 1)
+    band = ((col <= row) & (row - col < window)).astype(jnp.bfloat16)
+    sums = jnp.dot(band, here, preferred_element_type=jnp.float32)
+    behind = lax.broadcasted_iota(jnp.int32, (rows, span), 0) + span
+    behind = behind - lax.broadcasted_iota(jnp.int32, (rows, span), 1)
+    sums = sums + jnp.dot(
+        (behind < window).astype(jnp.bfloat16), normed(rim_ref), preferred_element_type=jnp.float32
+    )
+    position = sp_index * rows + lax.broadcasted_iota(jnp.int32, (rows, 1), 0)
+    divisor = jnp.minimum(position + 1, window).astype(jnp.float32)
+    pooled = (sums / divisor - here.astype(jnp.float32)).astype(jnp.bfloat16)
+    mixed = jnp.dot(pooled, weight_ref[...], preferred_element_type=jnp.float32) * scale_ref[...]
+    own = pl.ds(pl.multiple_of(tp_index * col_count, col_count), col_count)
+    stream = x_ref[:, own].astype(jnp.float32)
+    after = (stream + mixed.astype(jnp.bfloat16).astype(jnp.float32)).astype(jnp.bfloat16)
+    after_ref[...] = after
+
+    ids = ids_ref[...]
+    expert_index = lax.broadcasted_iota(jnp.int32, (experts, rows), 0)
+    named = [(ids[k : k + 1] == expert_index).astype(jnp.float32) for k in range(TOP_K)]
+    earlier = ((row // ROWS == col // ROWS) & (row < col)).astype(jnp.bfloat16)
+    before = jnp.dot(
+        sum(named).astype(jnp.bfloat16), earlier, preferred_element_type=jnp.float32
+    )
+    slots = rows // ROWS * CAP
+    block = lax.broadcasted_iota(jnp.int32, (1, rows), 1) // ROWS * CAP
+    targets = []
+    for k in range(TOP_K):
+        slot = jnp.sum(before * named[k], axis=0, keepdims=True).astype(jnp.int32)
+        targets.append(ids[k : k + 1] * slots + block + slot)
+        target_ref[k : k + 1] = targets[k]
+    for first in range(0, experts * slots, rows):
+        place_here = row + first
+        chosen = (place_here == targets[0]) | (place_here == targets[1])
+        outgoing_ref[first : first + rows] = jnp.dot(
+            chosen.astype(jnp.bfloat16), after, preferred_element_type=jnp.float32
+        ).astype(jnp.bfloat16)
+
+
+def mixer(index, ids, x, rim, gain, weight, scale, experts):
+    rows = x.shape[0]
+    col_count = weight.shape[1]
+    slots = rows // ROWS * CAP
+    return pl.pallas_call(
+        functools.partial(mixer_kernel, experts),
+        out_shape=(
+            jax.ShapeDtypeStruct((experts * slots, col_count), jnp.bfloat16),
+            jax.ShapeDtypeStruct((rows, col_count), jnp.bfloat16),
+            jax.ShapeDtypeStruct((TOP_K, rows), jnp.int32),
+        ),
+        in_specs=[SCALARS] + [VECTORS] * 6,
+        out_specs=(VECTORS,) * 3,
+        compiler_params=pltpu.CompilerParams(vmem_limit_bytes=16 * 2**20),
+        cost_estimate=pl.CostEstimate(
+            flops=10**9, bytes_accessed=4 * x.size, transcendentals=rows
+        ),
+        name="mixer",
+    )(index, ids, x, rim, gain[None], weight, scale[None])
+
+
+def halves_kernel(left_ref, right_ref, upper_ref, lower_ref):
+    upper_ref[...] = left_ref[...]
+    lower_ref[...] = right_ref[...]
+
+
+def halves(left, right, steps=3):
+    total, width = left.shape
+    rows = total // 2 // steps
+    first = pl.BlockSpec((rows, width), lambda i: (i, 0))
+    second = pl.BlockSpec((rows, width), lambda i: (i + steps, 0))
+    half = jax.ShapeDtypeStruct((total // 2, width), left.dtype)
+    return pl.pallas_call(
+        halves_kernel,
+        out_shape=(half, half),
+        grid=(steps,),
+        in_specs=[first, second],
+        out_specs=(first, first),
+        compiler_params=pltpu.CompilerParams(vmem_limit_bytes=8 * 2**20),
+        cost_estimate=pl.CostEstimate(
+            flops=10**6, bytes_accessed=2 * left.size * 2, transcendentals=0
+        ),
+        name="halves",
+    )(left, right)
+
+
+def combine_kernel(returned_ref, target_ref, share_ref, after_ref, out_ref):
+    rows = after_ref.shape[0]
+    total = after_ref[...].astype(jnp.float32)
+    slot = lax.broadcasted_iota(jnp.int32, (rows, returned_ref.shape[0]), 1)
+    mix = 0.0
+    for k in range(TOP_K):
+        chosen = (slot == target_ref[:, k : k + 1]).astype(jnp.bfloat16)
+        picked = jnp.dot(chosen, returned_ref[...], preferred_element_type=jnp.float32)
+        mix = mix + share_ref[:, k : k + 1] * picked
+    out = (total + mix).astype(jnp.bfloat16)
+    for t in range(out_ref.shape[0]):
+        out_ref[t] = out
+
+
+def combine(returned, target, share, after, copies):
+    return pl.pallas_call(
+        combine_kernel,
+        out_shape=jax.ShapeDtypeStruct((copies, *after.shape), jnp.bfloat16),
+        in_specs=[VECTORS] * 4,
+        out_specs=VECTORS,
+        compiler_params=pltpu.CompilerParams(vmem_limit_bytes=16 * 2**20),
+        cost_estimate=pl.CostEstimate(
+            flops=4 * returned.size * after.shape[0], bytes_accessed=10**6, transcendentals=0
+        ),
+        name="combine",
+    )(returned, target, share, after)
+
+
+def assemble_kernel(columns_ref, out_ref, semaphores):
+    copies = []
     for t in range(columns_ref.shape[0]):
-        out_ref[:, t * LANES : (t + 1) * LANES] = columns_ref[t, here]
-
-
-def assemble(columns, rows=64):
+        target = out_ref.at[:, t * LANES : (t + 1) * LANES]
+        copies.append(pltpu.make_async_copy(columns_ref.at[t], target, semaphores.at[t]))
+    for copy in copies:
+        copy.start()
+    for copy in copies:
+        copy.wait()
+
+
+def assemble(columns):
     count, total, lanes = columns.shape
     return pl.pallas_call(
         assemble_kernel,
         out_shape=jax.ShapeDtypeStruct((total, count * lanes), columns.dtype),
-        grid=(total // rows,),
         in_specs=[VECTORS],
-        out_specs=pl.BlockSpec((rows, count * lanes), lambda i: (i, 0)),
+        out_specs=ANYWHERE,
+        scratch_shapes=[pltpu.SemaphoreType.DMA((count,))],
+        compiler_params=pltpu.CompilerParams(vmem_limit_bytes=4 * 2**20),
         name="assemble",
     )(columns)
 
@@ -171,67 +324,22 @@
     tp_index = lax.axis_index(TP)
     sp_index = lax.axis_index(SP)
     tok_count, width = residual_in.shape
-    group_width = width // GROUPS
     col_count = pool_weight.shape[1]
     slots = tok_count // ROWS * CAP
-    group_index = tp_index * col_count // group_width
+    group_index = tp_index * col_count * GROUPS // width
 
     own = jnp.concatenate([gate_weight[0].T, up_weight[0].T, down_weight[0]], axis=0)
     left = from_quad(own, 1)
     right = from_quad(own, -1)
     rim = from_behind(residual_in[tok_count - SPAN :], SP, 1)
 
-    def normed_group(rows):
-        rows = rows.astype(jnp.float32)
-        inverse = lax.rsqrt(jnp.mean(rows * rows, axis=-1, keepdims=True) + EPS)
-        part = lax.dynamic_slice_in_dim(rows, group_index * group_width, group_width, 1)
-        gain = lax.dynamic_slice_in_dim(mix_gain, group_index * group_width, group_width, 0)
-        return lax.reduce_precision(part * inverse * gain, 8, 7)
-
-    extended = jnp.concatenate([normed_group(rim), normed_group(residual_in)], axis=0)
-    window_sum, sums = (None, extended)
-    for step in range(GROUPS):
-        reach = 2**step
-        sums = sums[reach:] + sums[:-reach]
-        here = sums[sums.shape[0] - tok_count :]
-        window_sum = here if step == 0 else jnp.where(group_index == step, here, window_sum)
-    window = jnp.left_shift(2, group_index)
-    position = sp_index * tok_count + jnp.arange(tok_count, dtype=jnp.int32)
-    divisor = jnp.minimum(position + 1, window).astype(jnp.float32)
-    pooled = (window_sum / divisor[:, None] - extended[SPAN:]).astype(jnp.bfloat16)
-    mixed = (jnp.dot(pooled, pool_weight, preferred_element_type=jnp.float32) * pool_scale).astype(
-        jnp.bfloat16
+    index = jnp.stack([group_index, tp_index, sp_index]).astype(jnp.int32)
+    outgoing, after, target = mixer(
+        index, route_ids.T, residual_in, rim, mix_gain, pool_weight, pool_scale, sp_count
     )
-    stream = lax.dynamic_slice_in_dim(residual_in, tp_index * col_count, col_count, 1)
-    after = (stream.astype(jnp.float32) + mixed.astype(jnp.float32)).astype(jnp.bfloat16)
-
-    token = np.arange(tok_count)
-    earlier = (token[:, None] // ROWS == token[None, :] // ROWS) & (token[None, :] < token[:, None])
-    experts = jnp.arange(sp_count, dtype=jnp.int32)
-    named = [(route_ids[:, k : k + 1] == experts[None, :]).astype(jnp.float32) for k in range(TOP_K)]
-    before = jnp.dot(
-        jnp.asarray(earlier, jnp.bfloat16),
-        sum(named).astype(jnp.bfloat16),
-        preferred_element_type=jnp.float32,
-    )
-    slot = jnp.arange(sp_count * slots, dtype=jnp.int32)
-    block = jnp.asarray(token // ROWS * CAP, jnp.int32)
-    tables = []
-    for k in range(TOP_K):
-        slot_of = jnp.sum(before * named[k], axis=1).astype(jnp.int32)
-        target = route_ids[:, k] * slots + block + slot_of
-        tables.append(target[:, None] == slot[None, :])
-    outgoing = lax.dot_general(
-        (tables[0] | tables[1]).astype(jnp.bfloat16),
-        after,
-        (((0,), (0,)), ((), ())),
-        preferred_element_type=jnp.float32,
-    ).astype(jnp.bfloat16)
     outgoing = outgoing.reshape(sp_count, slots, col_count)
     arrived = lax.all_to_all(outgoing, SP, 0, 0, tiled=True)
-    half = own.shape[0] // 2
-    upper = left[:half]
-    lower = right[half:]
+    upper, lower = halves(left, right)
     upper = from_quad(upper, 1)
     lower = from_quad(lower, -1)
     arrived = arrived.reshape(sp_count * slots, col_count)
@@ -247,14 +355,7 @@
     returned = lax.all_to_all(
         expert_out.reshape(sp_count, slots, col_count), SP, 0, 0, tiled=True
     ).reshape(sp_count * slots, col_count)
-    weights = sum(
-        jnp.where(tables[k], route_weights[:, k : k + 1], 0.0) for k in range(TOP_K)
-    )
-    expert_mix = jnp.dot(
-        weights, returned.astype(jnp.float32), precision=lax.Precision.HIGHEST
-    )
-    out = (after.astype(jnp.float32) + expert_mix).astype(jnp.bfloat16)
-    copies = jnp.broadcast_to(out[None], (tp_count, *out.shape))
+    copies = combine(returned, target.T, route_weights, after, tp_count)
     columns = lax.all_to_all(copies, TP, 0, 0, tiled=True)
     return assemble(columns)
 

time: 170 us -> 167 us (0.982)
  local copies, waits for them, and re-layouts: 7.79 us -> 2.56 us
  Pallas kernels: 8.48 us -> 13.6 us
  other arithmetic: 7.84 us -> 2.94 us
  waiting for transfers between devices: 32.5 us -> 37.3 us
  matrix products: 3.63 us -> 0 us
  starting transfers between devices: 51.4 us -> 53.3 us
    pallas_call x0 -> x3, Pallas kernels: none -> 6.86 us  [the longest x1 4.09 us: halves(): pl.pallas_call(halves_kernel, out_shape=(half, half), grid=(steps,), in_s...]
    slice x5 -> x0, local copies, waits for them, and re-layouts: 5.39 us -> none  [the longest x1 2.67 us: layer(): upper = left[:half]]
    ppermute x1, waiting for transfers between devices: 0.01 us -> 3.82 us  [from_behind(): lax.ppermute(value, axis, [(source, source + steps) for source in range(f...]
    dot_general x4 -> x0, matrix products: 3.63 us -> none  [the longest x1 1.3 us: layer(): lax.dot_general((tables[0] | tables[1]).astype(jnp.bfloat16), after, (((0...]
    ppermute x4, waiting for transfers between devices: 0.01 us -> 3.28 us  [from_quad(): return lax.ppermute(value, ALL, pairs)]
    convert_element_type x3 -> x0, other arithmetic: 2.92 us -> none  [the longest x2 2.91 us: normed_group(): rows = rows.astype(jnp.float32)]
    all_to_all x1, waiting for transfers between devices: 10.3 us -> 8.26 us  [layer(): arrived = lax.all_to_all(outgoing, SP, 0, 0, tiled=True)]
    all_to_all x1, starting transfers between devices: 18.2 us -> 20 us  [layer(): lax.all_to_all(expert_out.reshape(sp_count, slots, col_count), SP, 0, 0,...]
  transfers between devices with their start and end apart: 7 -> 7, of which waited for: 2 -> 5; matrix products, arithmetic and copies ran while one was open for 9% -> 1% of each run, Pallas kernels for 0% -> 4%
where the time goes in v5:
time: 167 us; the launch traced here: 166 us
  blocking collectives  56.2 us (34%)
  starting transfers between devices  53.3 us (32%)
  waiting for transfers between devices  37.3 us (22%)
  Pallas kernels  13.6 us (8%)
  other arithmetic  2.94 us (2%)
  local copies, waits for them, and re-layouts  2.56 us (2%)
    all_to_all x2, blocking collectives, exchange(): lax.all_to_all(blocks, ALL, 0, 0, tiled=True, axis_index_groups=groups)  37.5 us
    all_to_all x1, waiting for transfers between devices, layer(): lax.all_to_all(expert_out.reshape(sp_count, slots, col_count), SP, 0, 0,...  22 us
    all_to_all x1, starting transfers between devices, layer(): lax.all_to_all(expert_out.reshape(sp_count, slots, col_count), SP, 0, 0,...  20 us
    all_to_all x1, blocking collectives, layer(): columns = lax.all_to_all(copies, TP, 0, 0, tiled=True)  18.7 us
    all_to_all x1, starting transfers between devices, layer(): arrived = lax.all_to_all(outgoing, SP, 0, 0, tiled=True)  14.7 us
    ppermute x4, starting transfers between devices, from_quad(): return lax.ppermute(value, ALL, pairs)  14 us
    all_to_all x1, waiting for transfers between devices, layer(): arrived = lax.all_to_all(outgoing, SP, 0, 0, tiled=True)  8.26 us
    pallas_call x1, Pallas kernels, expert(): pl.pallas_call(functools.partial(expert_kernel, side), out_shape=jax.Shap...  5.67 us
  transfers between devices with their start and end apart: 7, of which 5 were waited for; matrix products, arithmetic and copies ran while one was open for 1% of the time, Pallas kernels for 4%

profile of v5, /device:TPU:1, one launch (start us, length us, event | category | flops | bytes accessed | tf_op | source)
XLA Modules:
  0.0 166.1 jit_solution(6274032667736888170)
XLA Ops:
  0.0 0.0 copy-start.2
  0.0 0.0 copy-start.3
  0.0 0.0 copy-start.4
  0.0 0.0 copy-start.5
  0.0 2.0 %pad_maximum_fusion.refs_0_ = bf16[672,2048]{1,0:T(8,128)(2,1)S(1)} fusion(bf16[224,2048]{1,0:T(8,128)(2,1)} %bitcast.31, bf16[224,2048]{1,0:T(8,128)(2,1)} %bitcast.32, bf16[224,2048]{1,0:T(8,128)(2,1)} %bitcast.33), kind=kLoop, calls=%fused_computation | loop fusion | flops 8257536 | bytes 5505024 | tf_op jit(solution)/shard_map/concatenate | solution.py:331
  2.0 4.0 %collective-permute-start.1 = (bf16[672,2048]{1,0:T(8,128)(2,1)S(1)}, bf16[672,2048]{1,0:T(8,128)(2,1)}, u32[]{:S(2)}, u32[]{:S(2)}) collective-permute-start(bf16[672,2048]{1,0:T(8,128)(2,1)S(1)} %pad_maximum_fusion.refs_0_), channel_id=1, source_target_pairs={{0,1},{1,2},{2,3},{3,0},{4,5},{5,6},{6,7},{7,4},{8,9},{9,10},{10,1... | collective-permute-start | bytes 8257544 | tf_op jit(solution)/shard_map/ppermute | solution.py:46
  6.0 3.4 %collective-permute-start.2 = (bf16[672,2048]{1,0:T(8,128)(2,1)S(1)}, bf16[672,2048]{1,0:T(8,128)(2,1)}, u32[]{:S(2)}, u32[]{:S(2)}) collective-permute-start(bf16[672,2048]{1,0:T(8,128)(2,1)S(1)} %pad_maximum_fusion.refs_0_), channel_id=1, source_target_pairs={{0,3},{1,0},{2,1},{3,2},{4,7},{5,4},{6,5},{7,6},{8,11},{9,8},{10,9... | collective-permute-start | bytes 8257544 | tf_op jit(solution)/shard_map/ppermute | solution.py:46
  9.4 0.8 slice.3
  10.2 4.6 %collective-permute-start = (bf16[16,2048]{1,0:T(8,128)(2,1)S(1)}, bf16[16,2048]{1,0:T(8,128)(2,1)S(1)}, u32[]{:S(2)}, u32[]{:S(2)}) collective-permute-start(bf16[16,2048]{1,0:T(8,128)(2,1)S(1)} %slice.3), channel_id=1, source_target_pairs={{0,16},{16,32},{32,48},{48,64},{64,80},{80,96},{96,112},{112,128},... | collective-permute-start | bytes 196616 | tf_op jit(solution)/shard_map/ppermute | solution.py:29
  14.8 0.1 pad_add_fusion.index_ref
  14.9 3.8 %collective-permute-done.rim_ref = bf16[16,2048]{1,0:T(8,128)(2,1)S(1)} collective-permute-done((bf16[16,2048]{1,0:T(8,128)(2,1)S(1)}, bf16[16,2048]{1,0:T(8,128)(2,1)S(1)}, u32[]{:S(2)}, u32[]{:S(2)}) %collective-permute-start) | collective-permute-done | bytes 65568 | tf_op jit(solution)/shard_map/ppermute | solution.py:29
  18.7 0.0 copy-done.2
  18.7 0.0 copy-done.3
  18.7 0.0 copy-done.4
  18.7 0.0 copy-done.5
  18.8 0.0 copy-start.1
  18.8 1.2 copy-done.1
  20.0 2.3 %mixer.1 = (bf16[1024,128]{1,0:T(8,128)(2,1)}, bf16[256,128]{1,0:T(8,128)(2,1)S(1)}, s32[2,256]{1,0:T(2,128)S(1)}) custom-call(s32[3]{0:T(128)S(1)} %pad_add_fusion.index_ref, s32[2,256]{1,0:T(2,128)S(1)} %bitcast.26, bf16[256,2048]{1,0:T(8,128)(2,1)S(1)} %copy-done.1, bf16[16,2048]{1,0:T(8,128)(2,1)S(1)} %collective-permute-done.rim_ref, ...), custom_call_target="tpu_custom_call" | custom-call | flops 1000000000 | bytes 2097152 | tf_op jit(solution)/shard_map/mixer/pallas_call | solution.py:216
  22.2 14.7 %all-to-all-start = ((bf16[32,32,128]{2,1,0:T(8,128)(2,1)}), bf16[32,32,128]{2,1,0:T(8,128)(2,1)S(1)}, u32[]{:S(2)}, u32[]{:S(2)}) async-start(bf16[32,32,128]{2,1,0:T(8,128)(2,1)} %bitcast.7), calls=%async_computation | async-start | bytes 524288 | tf_op jit(solution)/shard_map/all_to_all | solution.py:341
  36.9 1.3 collective-permute-done.1.left_ref.refs_1_
  38.3 1.9 %collective-permute-done.2.right_ref.refs_2_ = bf16[672,2048]{1,0:T(8,128)(2,1)} collective-permute-done((bf16[672,2048]{1,0:T(8,128)(2,1)S(1)}, bf16[672,2048]{1,0:T(8,128)(2,1)}, u32[]{:S(2)}, u32[]{:S(2)}) %collective-permute-start.2) | collective-permute-done | bytes 2752544 | tf_op jit(solution)/shard_map/ppermute | solution.py:46
  40.2 4.1 %halves.1 = (bf16[336,2048]{1,0:T(8,128)(2,1)}, bf16[336,2048]{1,0:T(8,128)(2,1)}) custom-call(bf16[672,2048]{1,0:T(8,128)(2,1)} %collective-permute-done.1.left_ref.refs_1_, bf16[672,2048]{1,0:T(8,128)(2,1)} %collective-permute-done.2.right_ref.refs_2_), custom_call_target="tpu_custom_call" | custom-call | flops 1000000 | bytes 5505024 | tf_op jit(solution)/shard_map/halves/pallas_call | solution.py:244
  44.3 0.0 copy-start
  44.3 3.3 %collective-permute-start.3 = (bf16[336,2048]{1,0:T(8,128)(2,1)}, bf16[336,2048]{1,0:T(8,128)(2,1)}, u32[]{:S(2)}, u32[]{:S(2)}) collective-permute-start(bf16[336,2048]{1,0:T(8,128)(2,1)} %get-tuple-element.11), channel_id=1, source_target_pairs={{0,1},{1,2},{2,3},{3,0},{4,5},{5,6},{6,7},{7,4},{8,9},{9,10},{10,1... | collective-permute-start | bytes 4128776 | tf_op jit(solution)/shard_map/ppermute | solution.py:46
  47.6 3.3 %collective-permute-start.4 = (bf16[336,2048]{1,0:T(8,128)(2,1)}, bf16[336,2048]{1,0:T(8,128)(2,1)}, u32[]{:S(2)}, u32[]{:S(2)}) collective-permute-start(bf16[336,2048]{1,0:T(8,128)(2,1)} %get-tuple-element.12), channel_id=1, source_target_pairs={{0,3},{1,0},{2,1},{3,2},{4,7},{5,4},{6,5},{7,6},{8,11},{9,8},{10,9... | collective-permute-start | bytes 4128776 | tf_op jit(solution)/shard_map/ppermute | solution.py:46
  50.9 8.3 %all-to-all-done = bf16[32,32,128]{2,1,0:T(8,128)(2,1)S(1)} async-done(((bf16[32,32,128]{2,1,0:T(8,128)(2,1)}), bf16[32,32,128]{2,1,0:T(8,128)(2,1)S(1)}, u32[]{:S(2)}, u32[]{:S(2)}) %all-to-all-start) | async-done | bytes 262176 | tf_op jit(solution)/shard_map/all_to_all | solution.py:341
  59.2 0.2 broadcast_in_dim.19
  59.4 21.9 %all_to_all.25.x_ref = bf16[16,256,128]{2,1,0:T(8,128)(2,1)S(1)} all-to-all(bf16[16,256,128]{2,1,0:T(8,128)(2,1)S(1)} %bitcast.28), channel_id=1, replica_groups={{0,1,2,3,4,5,6,7,8,9,10,11,12,13,14,15},{16,20,24,28,17,21,25,29,18,22,..., dimensions={0} | all-to-all | bytes 2097152 | tf_op jit(solution)/shard_map/all_to_all | solution.py:51
  81.3 0.0 collective-permute-done.3.refs_3_
  81.3 0.0 collective-permute-done.4.refs_4_
  81.3 0.0 copy-done
  81.4 5.7 %expert.1 = bf16[16,256,128]{2,1,0:T(8,128)(2,1)S(1)} custom-call(s32[1]{0:T(128)} %bitcast.core_ref, bf16[16,256,128]{2,1,0:T(8,128)(2,1)S(1)} %all_to_all.25.x_ref, f32[1,2048]{1,0:T(1,128)S(1)} %bitcast.24, bf16[672,2048]{1,0:T(8,128)(2,1)S(1)} %pad_maximum_fusion.refs_0_, bf16[672,2048]{1,0:T(8,128)(2,1)} %collective-permute-done.1.left_ref.refs_1_, ...), custom_call_target="tpu_custom_call" | custom-call | flops 2818572288 | bytes 11010048 | tf_op jit(solution)/shard_map/expert/pallas_call | solution.py:120
  87.0 0.0 copy-start.6
  87.0 15.5 %all_to_all.26 = bf16[16,256,128]{2,1,0:T(8,128)(2,1)S(1)} all-to-all(bf16[16,256,128]{2,1,0:T(8,128)(2,1)S(1)} %expert.1), channel_id=1, replica_groups={{0,1,2,3,4,5,6,7,8,9,10,11,12,13,14,15},{16,20,24,28,17,21,25,29,18,22,..., dimensions={0} | all-to-all | bytes 2097152 | tf_op jit(solution)/shard_map/all_to_all | solution.py:51
  102.6 0.9 reduce_sum.12
  103.5 20.0 %all-to-all-start.3 = ((bf16[32,32,128]{2,1,0:T(8,128)(2,1)}), bf16[32,32,128]{2,1,0:T(8,128)(2,1)S(1)}, u32[]{:S(2)}, u32[]{:S(2)}) async-start(bf16[32,32,128]{2,1,0:T(8,128)(2,1)} %bitcast.17), calls=%async_computation.3 | async-start | bytes 524288 | tf_op jit(solution)/shard_map/all_to_all | solution.py:355
  123.5 0.0 copy-done.6
  123.5 0.1 copy.12.share_ref
  123.7 0.1 copy.11
  123.8 22.0 %all-to-all-done.3 = bf16[32,32,128]{2,1,0:T(8,128)(2,1)S(1)} async-done(((bf16[32,32,128]{2,1,0:T(8,128)(2,1)}), bf16[32,32,128]{2,1,0:T(8,128)(2,1)S(1)}, u32[]{:S(2)}, u32[]{:S(2)}) %all-to-all-start.3) | async-done | bytes 262176 | tf_op jit(solution)/shard_map/all_to_all | solution.py:355
  145.8 0.5 combine.1
  146.3 18.7 %all_to_all.27.columns_ref = bf16[16,256,128]{2,1,0:T(8,128)(2,1)S(1)} all-to-all(bf16[16,256,128]{2,1,0:T(8,128)(2,1)S(1)} %combine.1), channel_id=1, replica_groups=mesh['z'=16,'c'=2,'y'=4,'x'=4] {'y','x'}, dimensions={0} | all-to-all | bytes 2097152 | tf_op jit(solution)/shard_map/all_to_all | solution.py:359
  165.0 1.1 assemble.1
Async XLA Ops:
  0.0 18.7 %copy-start.2 = (bf16[512,128]{1,0:T(8,128)(2,1)S(1)}, bf16[512,128]{1,0:T(8,128)(2,1)}, u32[]{:S(2)}) copy-start(bf16[512,128]{1,0:T(8,128)(2,1)} %weight_ref.1) | copy-start | bytes 393220
  0.0 18.7 %copy-start.3 = (f32[2048]{0:T(1024)S(1)}, f32[2048]{0:T(1024)}, u32[]{:S(2)}) copy-start(f32[2048]{0:T(1024)} %param.11) | copy-start | bytes 24580
  0.0 18.7 %copy-start.4 = (s32[256,2]{0,1:T(2,128)S(1)}, s32[256,2]{0,1:T(2,128)}, u32[]{:S(2)}) copy-start(s32[256,2]{0,1:T(2,128)} %param.15) | copy-start | bytes 6148
  0.0 18.7 %copy-start.5 = (f32[128]{0:T(128)S(1)}, f32[128]{0:T(128)}, u32[]{:S(2)}) copy-start(f32[128]{0:T(128)} %param.13) | copy-start | bytes 1540
  2.0 36.3 %collective-permute-start.1 = (bf16[672,2048]{1,0:T(8,128)(2,1)S(1)}, bf16[672,2048]{1,0:T(8,128)(2,1)}, u32[]{:S(2)}, u32[]{:S(2)}) collective-permute-start(bf16[672,2048]{1,0:T(8,128)(2,1)S(1)} %pad_maximum_fusion.refs_0_), channel_id=1, source_target_pairs={{0,1},{1,2},{2,3},{3,0},{4,5},{5,6},{6,7},{7,4},{8,9},{9,10},{10,1... | collective-permute-start | bytes 8257544 | tf_op jit(solution)/shard_map/ppermute | solution.py:46
  6.0 34.2 %collective-permute-start.2 = (bf16[672,2048]{1,0:T(8,128)(2,1)S(1)}, bf16[672,2048]{1,0:T(8,128)(2,1)}, u32[]{:S(2)}, u32[]{:S(2)}) collective-permute-start(bf16[672,2048]{1,0:T(8,128)(2,1)S(1)} %pad_maximum_fusion.refs_0_), channel_id=1, source_target_pairs={{0,3},{1,0},{2,1},{3,2},{4,7},{5,4},{6,5},{7,6},{8,11},{9,8},{10,9... | collective-permute-start | bytes 8257544 | tf_op jit(solution)/shard_map/ppermute | solution.py:46
  10.2 8.5 %collective-permute-start = (bf16[16,2048]{1,0:T(8,128)(2,1)S(1)}, bf16[16,2048]{1,0:T(8,128)(2,1)S(1)}, u32[]{:S(2)}, u32[]{:S(2)}) collective-permute-start(bf16[16,2048]{1,0:T(8,128)(2,1)S(1)} %slice.3), channel_id=1, source_target_pairs={{0,16},{16,32},{32,48},{48,64},{64,80},{80,96},{96,112},{112,128},... | collective-permute-start | bytes 196616 | tf_op jit(solution)/shard_map/ppermute | solution.py:29
  18.8 1.2 copy-start.1
  22.2 36.9 %all-to-all-start = ((bf16[32,32,128]{2,1,0:T(8,128)(2,1)}), bf16[32,32,128]{2,1,0:T(8,128)(2,1)S(1)}, u32[]{:S(2)}, u32[]{:S(2)}) async-start(bf16[32,32,128]{2,1,0:T(8,128)(2,1)} %bitcast.7), calls=%async_computation | async-start | bytes 524288 | tf_op jit(solution)/shard_map/all_to_all | solution.py:341
  44.3 37.1 %copy-start = (f32[2048]{0:T(1024)S(1)}, f32[2048]{0:T(1024)}, u32[]{:S(2)}) copy-start(f32[2048]{0:T(1024)} %param.14) | copy-start | bytes 24580
  44.3 37.0 %collective-permute-start.3 = (bf16[336,2048]{1,0:T(8,128)(2,1)}, bf16[336,2048]{1,0:T(8,128)(2,1)}, u32[]{:S(2)}, u32[]{:S(2)}) collective-permute-start(bf16[336,2048]{1,0:T(8,128)(2,1)} %get-tuple-element.11), channel_id=1, source_target_pairs={{0,1},{1,2},{2,3},{3,0},{4,5},{5,6},{6,7},{7,4},{8,9},{9,10},{10,1... | collective-permute-start | bytes 4128776 | tf_op jit(solution)/shard_map/ppermute | solution.py:46
  47.6 33.7 %collective-permute-start.4 = (bf16[336,2048]{1,0:T(8,128)(2,1)}, bf16[336,2048]{1,0:T(8,128)(2,1)}, u32[]{:S(2)}, u32[]{:S(2)}) collective-permute-start(bf16[336,2048]{1,0:T(8,128)(2,1)} %get-tuple-element.12), channel_id=1, source_target_pairs={{0,3},{1,0},{2,1},{3,2},{4,7},{5,4},{6,5},{7,6},{8,11},{9,8},{10,9... | collective-permute-start | bytes 4128776 | tf_op jit(solution)/shard_map/ppermute | solution.py:46
  87.0 36.5 %copy-start.6 = (f32[256,2]{0,1:T(2,128)S(1)}, f32[256,2]{0,1:T(2,128)}, u32[]{:S(2)}) copy-start(f32[256,2]{0,1:T(2,128)} %param.16) | copy-start | bytes 6148
  103.5 42.3 %all-to-all-start.3 = ((bf16[32,32,128]{2,1,0:T(8,128)(2,1)}), bf16[32,32,128]{2,1,0:T(8,128)(2,1)S(1)}, u32[]{:S(2)}, u32[]{:S(2)}) async-start(bf16[32,32,128]{2,1,0:T(8,128)(2,1)} %bitcast.17), calls=%async_computation.3 | async-start | bytes 524288 | tf_op jit(solution)/shard_map/all_to_all | solution.py:355

commit v6 on v5

--- a/solution.py
+++ b/solution.py
@@ -56,13 +56,14 @@
 
 
 def expert_kernel(side, core_ref, x_ref, gain_ref, *refs):
-    pieces = (len(refs) - 3) // 2
+    pieces = (len(refs) - 3) // 3 * 2
     sources, out_ref, normed_ref = (refs[:pieces], refs[pieces], refs[pieces + 1])
-    weights, semaphores = (refs[pieces + 2 : 2 * pieces + 2], refs[-1])
-    copies = [
-        pltpu.make_async_copy(source, target, semaphores.at[i])
-        for i, (source, target) in enumerate(zip(sources, weights))
-    ]
+    weights, semaphores = (refs[pieces + 2 : -1], refs[-1])
+    copies = []
+    for i, source in enumerate(sources):
+        height = source.shape[0]
+        target = weights[i // 2].at[i % 2 * height : (i % 2 + 1) * height]
+        copies.append(pltpu.make_async_copy(source, target, semaphores.at[i]))
     for copy in copies:
         copy.start()
     count, rows, lanes = x_ref.shape
@@ -79,19 +80,11 @@
     contract = (((1,), (1,)), ((), ()))
     normed = normed_ref[...]
     hidden, downs = ([], [])
-    for i in range(pieces - 1):
-        copies[i].wait()
-        gate_rows, up_rows = (weights[i][:units], None)
-        if i < pieces - 2:
-            up_rows = weights[i][units : 2 * units]
-            downs.append(weights[i].at[2 * units :])
-        else:
-            copies[i + 1].wait()
-            cut = weights[i].shape[0]
-            up_rows = jnp.concatenate(
-                [weights[i][units:], weights[i + 1][: 2 * units - cut]], axis=0
-            )
-            downs.append(weights[i + 1].at[2 * units - cut :])
+    for i, ref in enumerate(weights):
+        copies[2 * i].wait()
+        copies[2 * i + 1].wait()
+        gate_rows, up_rows = (ref[:units], ref[units : 2 * units])
+        downs.append(ref.at[2 * units :])
         gate = lax.dot_general(normed, gate_rows, contract, preferred_element_type=jnp.float32)
         up = lax.dot_general(normed, up_rows, contract, preferred_element_type=jnp.float32)
         hidden.append((gate * (1.0 / (1.0 + jnp.exp(-gate))) * up).astype(jnp.bfloat16))
@@ -116,14 +109,16 @@
 def expert(blocks, core, gain, weights, side):
     count, rows, lanes = blocks.shape
     width = count * lanes
-    units = weights[0].shape[0] // 3
+    slices = len(weights) // 2
+    height = 2 * weights[0].shape[0]
+    units = height // 3
     return pl.pallas_call(
         functools.partial(expert_kernel, side),
         out_shape=jax.ShapeDtypeStruct(blocks.shape, jnp.bfloat16),
         in_specs=[SCALARS, VECTORS, VECTORS] + [ANYWHERE] * len(weights),
         out_specs=VECTORS,
         scratch_shapes=[pltpu.VMEM((rows, width), jnp.bfloat16)]
-        + [pltpu.VMEM(w.shape, w.dtype) for w in weights]
+        + [pltpu.VMEM((height, width), jnp.bfloat16)] * slices
         + [pltpu.SemaphoreType.DMA((len(weights),))],
         compiler_params=pltpu.CompilerParams(vmem_limit_bytes=32 * 2**20),
         cost_estimate=pl.CostEstimate(
@@ -230,31 +225,6 @@
     )(index, ids, x, rim, gain[None], weight, scale[None])
 
 
-def halves_kernel(left_ref, right_ref, upper_ref, lower_ref):
-    upper_ref[...] = left_ref[...]
-    lower_ref[...] = right_ref[...]
-
-
-def halves(left, right, steps=3):
-    total, width = left.shape
-    rows = total // 2 // steps
-    first = pl.BlockSpec((rows, width), lambda i: (i, 0))
-    second = pl.BlockSpec((rows, width), lambda i: (i + steps, 0))
-    half = jax.ShapeDtypeStruct((total // 2, width), left.dtype)
-    return pl.pallas_call(
-        halves_kernel,
-        out_shape=(half, half),
-        grid=(steps,),
-        in_specs=[first, second],
-        out_specs=(first, first),
-        compiler_params=pltpu.CompilerParams(vmem_limit_bytes=8 * 2**20),
-        cost_estimate=pl.CostEstimate(
-            flops=10**6, bytes_accessed=2 * left.size * 2, transcendentals=0
-        ),
-        name="halves",
-    )(left, right)
-
-
 def combine_kernel(returned_ref, target_ref, share_ref, after_ref, out_ref):
     rows = after_ref.shape[0]
     total = after_ref[...].astype(jnp.float32)
@@ -328,9 +298,12 @@
     slots = tok_count // ROWS * CAP
     group_index = tp_index * col_count * GROUPS // width
 
-    own = jnp.concatenate([gate_weight[0].T, up_weight[0].T, down_weight[0]], axis=0)
-    left = from_quad(own, 1)
-    right = from_quad(own, -1)
+    middle = up_weight.shape[2] // 2
+    up_t = up_weight[0].T
+    top = jnp.concatenate([gate_weight[0].T, up_t[:middle]], axis=0)
+    bottom = jnp.concatenate([up_t[middle:], down_weight[0]], axis=0)
+    left_top, right_bottom = (from_quad(top, 1), from_quad(bottom, -1))
+    left_bottom, right_top = (from_quad(bottom, 1), from_quad(top, -1))
     rim = from_behind(residual_in[tok_count - SPAN :], SP, 1)
 
     index = jnp.stack([group_index, tp_index, sp_index]).astype(jnp.int32)
@@ -339,17 +312,14 @@
     )
     outgoing = outgoing.reshape(sp_count, slots, col_count)
     arrived = lax.all_to_all(outgoing, SP, 0, 0, tiled=True)
-    upper, lower = halves(left, right)
-    upper = from_quad(upper, 1)
-    lower = from_quad(lower, -1)
-    arrived = arrived.reshape(sp_count * slots, col_count)
+    far_top, far_bottom = (from_quad(left_top, 1), from_quad(right_bottom, -1))
 
     side = lax.axis_size("x")
     core = lax.axis_index("c").astype(jnp.int32).reshape(1)
     quarter = arrived.reshape(1, side, -1, col_count)
     quarter = jnp.broadcast_to(quarter, (side, *quarter.shape[1:]))
     gathered = exchange(quarter.reshape(tp_count, -1, col_count))
-    term = expert(gathered, core, ffn_gain, [own, left, right, upper, lower], side)
+    term = expert(gathered, core, ffn_gain, [top, bottom, left_top, left_bottom, right_top, right_bottom, far_top, far_bottom], side)
     summed = exchange(term).reshape(quarter.shape)
     expert_out = jnp.sum(summed.astype(jnp.float32), axis=0).astype(jnp.bfloat16)
     returned = lax.all_to_all(

time: 167 us -> 171 us (1.024)
  blocking collectives: 56.2 us -> 38 us
  waiting for transfers between devices: 37.3 us -> 53.5 us
  starting transfers between devices: 53.3 us -> 61.9 us
  Pallas kernels: 13.6 us -> 10.7 us
  local copies, waits for them, and re-layouts: 2.56 us -> 5 us
  other arithmetic: 2.94 us -> 1.21 us
    all_to_all x0 -> x1, waiting for transfers between devices: none -> 18.5 us  [exchange(): lax.all_to_all(blocks, ALL, 0, 0, tiled=True, axis_index_groups=groups)]
    all_to_all x2 -> x1, blocking collectives: 37.5 us -> 19.3 us  [exchange(): lax.all_to_all(blocks, ALL, 0, 0, tiled=True, axis_index_groups=groups)]
    ppermute x4 -> x6, starting transfers between devices: 14 us -> 20.6 us  [from_quad(): return lax.ppermute(value, ALL, pairs)]
    all_to_all x0 -> x1, starting transfers between devices: none -> 5.73 us  [exchange(): lax.all_to_all(blocks, ALL, 0, 0, tiled=True, axis_index_groups=groups)]
    pallas_call x1 -> x0, Pallas kernels: 4.09 us -> none  [halves(): pl.pallas_call(halves_kernel, out_shape=(half, half), grid=(steps,), in_s...]
    all_to_all x1, starting transfers between devices: 20 us -> 16.3 us  [layer(): lax.all_to_all(expert_out.reshape(sp_count, slots, col_count), SP, 0, 0,...]
    ppermute x4 -> x6, waiting for transfers between devices: 3.28 us -> 0.02 us  [from_quad(): return lax.ppermute(value, ALL, pairs)]
    concatenate x1 -> x2, other arithmetic: 1.96 us -> 0.23 us  [the longest x1 0.14 us: layer(): top = jnp.concatenate([gate_weight[0].T, up_t[:middle]], axis=0)]
  transfers between devices with their start and end apart: 7 -> 10, of which waited for: 5 -> 4; matrix products, arithmetic and copies ran while one was open for 1% -> 1% of each run, Pallas kernels for 4% -> 1%
where the time goes in v6:
time: 171 us
  starting transfers between devices  61.9 us (36%)
  waiting for transfers between devices  53.5 us (31%)
  blocking collectives  38 us (22%)
  Pallas kernels  10.7 us (6%)
  local copies, waits for them, and re-layouts  5 us (3%)
    all_to_all x1, waiting for transfers between devices, layer(): lax.all_to_all(expert_out.reshape(sp_count, slots, col_count), SP, 0, 0,...  22 us
    ppermute x6, starting transfers between devices, from_quad(): return lax.ppermute(value, ALL, pairs)  20.6 us
    all_to_all x1, blocking collectives, exchange(): lax.all_to_all(blocks, ALL, 0, 0, tiled=True, axis_index_groups=groups)  19.3 us
    all_to_all x1, blocking collectives, layer(): columns = lax.all_to_all(copies, TP, 0, 0, tiled=True)  18.7 us
    all_to_all x1, waiting for transfers between devices, exchange(): lax.all_to_all(blocks, ALL, 0, 0, tiled=True, axis_index_groups=groups)  18.5 us
    all_to_all x1, starting transfers between devices, layer(): lax.all_to_all(expert_out.reshape(sp_count, slots, col_count), SP, 0, 0,...  16.3 us
    all_to_all x1, starting transfers between devices, layer(): arrived = lax.all_to_all(outgoing, SP, 0, 0, tiled=True)  14.7 us
    all_to_all x1, waiting for transfers between devices, layer(): arrived = lax.all_to_all(outgoing, SP, 0, 0, tiled=True)  9.15 us
  transfers between devices with their start and end apart: 10, of which 4 were waited for; matrix products, arithmetic and copies ran while one was open for 1% of the time, Pallas kernels for 1%

profile of v6, /device:TPU:1, one launch (start us, length us, event | category | flops | bytes accessed | tf_op | source)
XLA Modules:
  0.0 170.6 jit_solution(3539855865948002931)
XLA Ops:
  0.0 1.3 fusion
  1.3 0.1 copy-done.6
  1.5 0.1 pad_maximum_fusion.refs_0_
  1.6 4.2 %collective-permute-start.1 = (bf16[336,2048]{1,0:T(8,128)(2,1)S(1)}, bf16[336,2048]{1,0:T(8,128)(2,1)}, u32[]{:S(2)}, u32[]{:S(2)}) collective-permute-start(bf16[336,2048]{1,0:T(8,128)(2,1)S(1)} %pad_maximum_fusion.refs_0_), channel_id=1, source_target_pairs={{0,1},{1,2},{2,3},{3,0},{4,5},{5,6},{6,7},{7,4},{8,9},{9,10},{10,1... | collective-permute-start | bytes 4128776 | tf_op jit(solution)/shard_map/ppermute | solution.py:46
  5.8 0.0 copy-done.7
  5.8 0.0 copy-start.2
  5.8 0.0 copy-start.3
  5.8 0.0 copy-start.4
  5.8 0.0 copy-start.5
  5.8 0.1 pad_maximum_fusion.1.refs_1_
  5.9 3.4 %collective-permute-start.4 = (bf16[336,2048]{1,0:T(8,128)(2,1)S(1)}, bf16[336,2048]{1,0:T(8,128)(2,1)}, u32[]{:S(2)}, u32[]{:S(2)}) collective-permute-start(bf16[336,2048]{1,0:T(8,128)(2,1)S(1)} %pad_maximum_fusion.1.refs_1_), channel_id=1, source_target_pairs={{0,3},{1,0},{2,1},{3,2},{4,7},{5,4},{6,5},{7,6},{8,11},{9,8},{10,9... | collective-permute-start | bytes 4128776 | tf_op jit(solution)/shard_map/ppermute | solution.py:46
  9.3 0.8 slice.9
  10.1 4.6 %collective-permute-start = (bf16[16,2048]{1,0:T(8,128)(2,1)S(1)}, bf16[16,2048]{1,0:T(8,128)(2,1)S(1)}, u32[]{:S(2)}, u32[]{:S(2)}) collective-permute-start(bf16[16,2048]{1,0:T(8,128)(2,1)S(1)} %slice.9), channel_id=1, source_target_pairs={{0,16},{16,32},{32,48},{48,64},{64,80},{80,96},{96,112},{112,128},... | collective-permute-start | bytes 196616 | tf_op jit(solution)/shard_map/ppermute | solution.py:29
  14.8 0.1 pad_add_fusion.index_ref
  14.8 3.8 %collective-permute-done.rim_ref = bf16[16,2048]{1,0:T(8,128)(2,1)S(1)} collective-permute-done((bf16[16,2048]{1,0:T(8,128)(2,1)S(1)}, bf16[16,2048]{1,0:T(8,128)(2,1)S(1)}, u32[]{:S(2)}, u32[]{:S(2)}) %collective-permute-start) | collective-permute-done | bytes 65568 | tf_op jit(solution)/shard_map/ppermute | solution.py:29
  18.7 0.0 copy-done.2
  18.7 0.0 copy-done.3
  18.7 0.0 copy-done.4
  18.7 0.0 copy-done.5
  18.7 0.0 copy-start.1
  18.7 1.2 copy-done.1
  19.9 2.3 %mixer.1 = (bf16[1024,128]{1,0:T(8,128)(2,1)}, bf16[256,128]{1,0:T(8,128)(2,1)S(1)}, s32[2,256]{1,0:T(2,128)S(1)}) custom-call(s32[3]{0:T(128)S(1)} %pad_add_fusion.index_ref, s32[2,256]{1,0:T(2,128)S(1)} %bitcast.26, bf16[256,2048]{1,0:T(8,128)(2,1)S(1)} %copy-done.1, bf16[16,2048]{1,0:T(8,128)(2,1)S(1)} %collective-permute-done.rim_ref, ...), custom_call_target="tpu_custom_call" | custom-call | flops 1000000000 | bytes 2097152 | tf_op jit(solution)/shard_map/mixer/pallas_call | solution.py:211
  22.2 14.7 %all-to-all-start = ((bf16[32,32,128]{2,1,0:T(8,128)(2,1)}), bf16[32,32,128]{2,1,0:T(8,128)(2,1)S(1)}, u32[]{:S(2)}, u32[]{:S(2)}) async-start(bf16[32,32,128]{2,1,0:T(8,128)(2,1)} %bitcast.7), calls=%async_computation | async-start | bytes 524288 | tf_op jit(solution)/shard_map/all_to_all | solution.py:314
  36.9 3.2 %collective-permute-start.2 = (bf16[336,2048]{1,0:T(8,128)(2,1)S(1)}, bf16[336,2048]{1,0:T(8,128)(2,1)}, u32[]{:S(2)}, u32[]{:S(2)}) collective-permute-start(bf16[336,2048]{1,0:T(8,128)(2,1)S(1)} %pad_maximum_fusion.1.refs_1_), channel_id=1, source_target_pairs={{0,1},{1,2},{2,3},{3,0},{4,5},{5,6},{6,7},{7,4},{8,9},{9,10},{10,1... | collective-permute-start | bytes 4128776 | tf_op jit(solution)/shard_map/ppermute | solution.py:46
  40.1 3.4 %collective-permute-start.3 = (bf16[336,2048]{1,0:T(8,128)(2,1)S(1)}, bf16[336,2048]{1,0:T(8,128)(2,1)}, u32[]{:S(2)}, u32[]{:S(2)}) collective-permute-start(bf16[336,2048]{1,0:T(8,128)(2,1)S(1)} %pad_maximum_fusion.refs_0_), channel_id=1, source_target_pairs={{0,3},{1,0},{2,1},{3,2},{4,7},{5,4},{6,5},{7,6},{8,11},{9,8},{10,9... | collective-permute-start | bytes 4128776 | tf_op jit(solution)/shard_map/ppermute | solution.py:46
  43.4 0.0 collective-permute-done.1.refs_2_
  43.4 1.9 %collective-permute-start.5 = (bf16[336,2048]{1,0:T(8,128)(2,1)}, bf16[336,2048]{1,0:T(8,128)(2,1)}, u32[]{:S(2)}, u32[]{:S(2)}) collective-permute-start(bf16[336,2048]{1,0:T(8,128)(2,1)} %collective-permute-done.1.refs_2_), channel_id=1, source_target_pairs={{0,1},{1,2},{2,3},{3,0},{4,5},{5,6},{6,7},{7,4},{8,9},{9,10},{10,1... | collective-permute-start | bytes 4128776 | tf_op jit(solution)/shard_map/ppermute | solution.py:46
  45.4 0.0 collective-permute-done.4.refs_5_
  45.4 4.6 %collective-permute-start.6 = (bf16[336,2048]{1,0:T(8,128)(2,1)}, bf16[336,2048]{1,0:T(8,128)(2,1)}, u32[]{:S(2)}, u32[]{:S(2)}) collective-permute-start(bf16[336,2048]{1,0:T(8,128)(2,1)} %collective-permute-done.4.refs_5_), channel_id=1, source_target_pairs={{0,3},{1,0},{2,1},{3,2},{4,7},{5,4},{6,5},{7,6},{8,11},{9,8},{10,9... | collective-permute-start | bytes 4128776 | tf_op jit(solution)/shard_map/ppermute | solution.py:46
  50.0 9.1 %all-to-all-done = bf16[32,32,128]{2,1,0:T(8,128)(2,1)S(1)} async-done(((bf16[32,32,128]{2,1,0:T(8,128)(2,1)}), bf16[32,32,128]{2,1,0:T(8,128)(2,1)S(1)}, u32[]{:S(2)}, u32[]{:S(2)}) %all-to-all-start) | async-done | bytes 262176 | tf_op jit(solution)/shard_map/all_to_all | solution.py:314
  59.1 1.2 broadcast_in_dim.19
  60.3 5.7 %all-to-all-start.1 = ((bf16[16,256,128]{2,1,0:T(8,128)(2,1)}), bf16[16,256,128]{2,1,0:T(8,128)(2,1)}, u32[]{:S(2)}, u32[]{:S(2)}) async-start(bf16[16,256,128]{2,1,0:T(8,128)(2,1)} %bitcast.28), calls=%async_computation.1 | async-start | bytes 2097152 | tf_op jit(solution)/shard_map/all_to_all | solution.py:51
  66.0 0.0 collective-permute-done.2.refs_3_
  66.0 0.0 collective-permute-done.3.refs_4_
  66.0 18.5 %all-to-all-done.1.x_ref = bf16[16,256,128]{2,1,0:T(8,128)(2,1)} async-done(((bf16[16,256,128]{2,1,0:T(8,128)(2,1)}), bf16[16,256,128]{2,1,0:T(8,128)(2,1)}, u32[]{:S(2)}, u32[]{:S(2)}) %all-to-all-start.1) | async-done | bytes 1048608 | tf_op jit(solution)/shard_map/all_to_all | solution.py:51
  84.6 0.0 collective-permute-done.5.refs_6_
  84.6 0.0 collective-permute-done.6.refs_7_
  84.6 0.0 copy-done
  84.6 6.9 %expert.1 = bf16[16,256,128]{2,1,0:T(8,128)(2,1)S(1)} custom-call(s32[1]{0:T(128)} %bitcast.core_ref, bf16[16,256,128]{2,1,0:T(8,128)(2,1)} %all-to-all-done.1.x_ref, f32[1,2048]{1,0:T(1,128)S(1)} %bitcast.24, bf16[336,2048]{1,0:T(8,128)(2,1)S(1)} %pad_maximum_fusion.refs_0_, bf16[336,2048]{1,0:T(8,128)(2,1)S(1)} %pad_maximum_fusion.1.refs_1_, ...), custom_call_target="tpu_custom_call" | custom-call | flops 2818572288 | bytes 11010048 | tf_op jit(solution)/shard_map/expert/pallas_call | solution.py:115
  91.5 19.3 %all_to_all.25 = bf16[16,256,128]{2,1,0:T(8,128)(2,1)S(1)} all-to-all(bf16[16,256,128]{2,1,0:T(8,128)(2,1)S(1)} %expert.1), channel_id=1, replica_groups={{0,1,2,3,4,5,6,7,8,9,10,11,12,13,14,15},{16,20,24,28,17,21,25,29,18,22,..., dimensions={0} | all-to-all | bytes 2097152 | tf_op jit(solution)/shard_map/all_to_all | solution.py:51
  110.8 0.9 reduce_sum.12
  111.7 16.3 %all-to-all-start.3 = ((bf16[32,32,128]{2,1,0:T(8,128)(2,1)}), bf16[32,32,128]{2,1,0:T(8,128)(2,1)S(1)}, u32[]{:S(2)}, u32[]{:S(2)}) async-start(bf16[32,32,128]{2,1,0:T(8,128)(2,1)} %bitcast.18), calls=%async_computation.3 | async-start | bytes 524288 | tf_op jit(solution)/shard_map/all_to_all | solution.py:325
  128.0 0.1 copy.12.share_ref
  128.2 0.1 copy.11
  128.3 22.0 %all-to-all-done.3 = bf16[32,32,128]{2,1,0:T(8,128)(2,1)S(1)} async-done(((bf16[32,32,128]{2,1,0:T(8,128)(2,1)}), bf16[32,32,128]{2,1,0:T(8,128)(2,1)S(1)}, u32[]{:S(2)}, u32[]{:S(2)}) %all-to-all-start.3) | async-done | bytes 262176 | tf_op jit(solution)/shard_map/all_to_all | solution.py:325
  150.3 0.5 combine.1
  150.8 18.7 %all_to_all.26.columns_ref = bf16[16,256,128]{2,1,0:T(8,128)(2,1)S(1)} all-to-all(bf16[16,256,128]{2,1,0:T(8,128)(2,1)S(1)} %combine.1), channel_id=1, replica_groups=mesh['z'=16,'c'=2,'y'=4,'x'=4] {'y','x'}, dimensions={0} | all-to-all | bytes 2097152 | tf_op jit(solution)/shard_map/all_to_all | solution.py:329
  169.5 1.1 assemble.1
  (5 shorter events, 0.0 us)
Async XLA Ops:
  0.0 1.5 copy-start.6
  1.5 4.3 %copy-start.7 = (bf16[1,224,2048]{2,1,0:T(8,128)(2,1)S(1)}, bf16[1,224,2048]{2,1,0:T(8,128)(2,1)}, u32[]{:S(2)}) copy-start(bf16[1,224,2048]{2,1,0:T(8,128)(2,1)} %param.19) | copy-start | bytes 2752516
  1.6 41.8 %collective-permute-start.1 = (bf16[336,2048]{1,0:T(8,128)(2,1)S(1)}, bf16[336,2048]{1,0:T(8,128)(2,1)}, u32[]{:S(2)}, u32[]{:S(2)}) collective-permute-start(bf16[336,2048]{1,0:T(8,128)(2,1)S(1)} %pad_maximum_fusion.refs_0_), channel_id=1, source_target_pairs={{0,1},{1,2},{2,3},{3,0},{4,5},{5,6},{6,7},{7,4},{8,9},{9,10},{10,1... | collective-permute-start | bytes 4128776 | tf_op jit(solution)/shard_map/ppermute | solution.py:46
  5.8 12.9 %copy-start.2 = (bf16[512,128]{1,0:T(8,128)(2,1)S(1)}, bf16[512,128]{1,0:T(8,128)(2,1)}, u32[]{:S(2)}) copy-start(bf16[512,128]{1,0:T(8,128)(2,1)} %weight_ref.1) | copy-start | bytes 393220
  5.8 12.9 %copy-start.3 = (f32[2048]{0:T(1024)S(1)}, f32[2048]{0:T(1024)}, u32[]{:S(2)}) copy-start(f32[2048]{0:T(1024)} %param.11) | copy-start | bytes 24580
  5.8 12.9 %copy-start.4 = (s32[256,2]{0,1:T(2,128)S(1)}, s32[256,2]{0,1:T(2,128)}, u32[]{:S(2)}) copy-start(s32[256,2]{0,1:T(2,128)} %param.15) | copy-start | bytes 6148
  5.8 12.9 %copy-start.5 = (f32[128]{0:T(128)S(1)}, f32[128]{0:T(128)}, u32[]{:S(2)}) copy-start(f32[128]{0:T(128)} %param.13) | copy-start | bytes 1540
  5.9 39.5 %collective-permute-start.4 = (bf16[336,2048]{1,0:T(8,128)(2,1)S(1)}, bf16[336,2048]{1,0:T(8,128)(2,1)}, u32[]{:S(2)}, u32[]{:S(2)}) collective-permute-start(bf16[336,2048]{1,0:T(8,128)(2,1)S(1)} %pad_maximum_fusion.1.refs_1_), channel_id=1, source_target_pairs={{0,3},{1,0},{2,1},{3,2},{4,7},{5,4},{6,5},{7,6},{8,11},{9,8},{10,9... | collective-permute-start | bytes 4128776 | tf_op jit(solution)/shard_map/ppermute | solution.py:46
  10.1 8.5 %collective-permute-start = (bf16[16,2048]{1,0:T(8,128)(2,1)S(1)}, bf16[16,2048]{1,0:T(8,128)(2,1)S(1)}, u32[]{:S(2)}, u32[]{:S(2)}) collective-permute-start(bf16[16,2048]{1,0:T(8,128)(2,1)S(1)} %slice.9), channel_id=1, source_target_pairs={{0,16},{16,32},{32,48},{48,64},{64,80},{80,96},{96,112},{112,128},... | collective-permute-start | bytes 196616 | tf_op jit(solution)/shard_map/ppermute | solution.py:29
  18.7 1.2 copy-start.1
  22.2 36.9 %all-to-all-start = ((bf16[32,32,128]{2,1,0:T(8,128)(2,1)}), bf16[32,32,128]{2,1,0:T(8,128)(2,1)S(1)}, u32[]{:S(2)}, u32[]{:S(2)}) async-start(bf16[32,32,128]{2,1,0:T(8,128)(2,1)} %bitcast.7), calls=%async_computation | async-start | bytes 524288 | tf_op jit(solution)/shard_map/all_to_all | solution.py:314
  36.9 29.2 %collective-permute-start.2 = (bf16[336,2048]{1,0:T(8,128)(2,1)S(1)}, bf16[336,2048]{1,0:T(8,128)(2,1)}, u32[]{:S(2)}, u32[]{:S(2)}) collective-permute-start(bf16[336,2048]{1,0:T(8,128)(2,1)S(1)} %pad_maximum_fusion.1.refs_1_), channel_id=1, source_target_pairs={{0,1},{1,2},{2,3},{3,0},{4,5},{5,6},{6,7},{7,4},{8,9},{9,10},{10,1... | collective-permute-start | bytes 4128776 | tf_op jit(solution)/shard_map/ppermute | solution.py:46
  40.1 26.0 %collective-permute-start.3 = (bf16[336,2048]{1,0:T(8,128)(2,1)S(1)}, bf16[336,2048]{1,0:T(8,128)(2,1)}, u32[]{:S(2)}, u32[]{:S(2)}) collective-permute-start(bf16[336,2048]{1,0:T(8,128)(2,1)S(1)} %pad_maximum_fusion.refs_0_), channel_id=1, source_target_pairs={{0,3},{1,0},{2,1},{3,2},{4,7},{5,4},{6,5},{7,6},{8,11},{9,8},{10,9... | collective-permute-start | bytes 4128776 | tf_op jit(solution)/shard_map/ppermute | solution.py:46
  43.4 41.2 %collective-permute-start.5 = (bf16[336,2048]{1,0:T(8,128)(2,1)}, bf16[336,2048]{1,0:T(8,128)(2,1)}, u32[]{:S(2)}, u32[]{:S(2)}) collective-permute-start(bf16[336,2048]{1,0:T(8,128)(2,1)} %collective-permute-done.1.refs_2_), channel_id=1, source_target_pairs={{0,1},{1,2},{2,3},{3,0},{4,5},{5,6},{6,7},{7,4},{8,9},{9,10},{10,1... | collective-permute-start | bytes 4128776 | tf_op jit(solution)/shard_map/ppermute | solution.py:46
  45.4 39.2 %collective-permute-start.6 = (bf16[336,2048]{1,0:T(8,128)(2,1)}, bf16[336,2048]{1,0:T(8,128)(2,1)}, u32[]{:S(2)}, u32[]{:S(2)}) collective-permute-start(bf16[336,2048]{1,0:T(8,128)(2,1)} %collective-permute-done.4.refs_5_), channel_id=1, source_target_pairs={{0,3},{1,0},{2,1},{3,2},{4,7},{5,4},{6,5},{7,6},{8,11},{9,8},{10,9... | collective-permute-start | bytes 4128776 | tf_op jit(solution)/shard_map/ppermute | solution.py:46
  60.3 24.3 %copy-start = (f32[2048]{0:T(1024)S(1)}, f32[2048]{0:T(1024)}, u32[]{:S(2)}) copy-start(f32[2048]{0:T(1024)} %param.14) | copy-start | bytes 24580
  60.3 24.3 %all-to-all-start.1 = ((bf16[16,256,128]{2,1,0:T(8,128)(2,1)}), bf16[16,256,128]{2,1,0:T(8,128)(2,1)}, u32[]{:S(2)}, u32[]{:S(2)}) async-start(bf16[16,256,128]{2,1,0:T(8,128)(2,1)} %bitcast.28), calls=%async_computation.1 | async-start | bytes 2097152 | tf_op jit(solution)/shard_map/all_to_all | solution.py:51
  110.8 17.2 %copy-start.8 = (f32[256,2]{0,1:T(2,128)S(1)}, f32[256,2]{0,1:T(2,128)}, u32[]{:S(2)}) copy-start(f32[256,2]{0,1:T(2,128)} %param.16) | copy-start | bytes 6148
  111.7 38.6 %all-to-all-start.3 = ((bf16[32,32,128]{2,1,0:T(8,128)(2,1)}), bf16[32,32,128]{2,1,0:T(8,128)(2,1)S(1)}, u32[]{:S(2)}, u32[]{:S(2)}) async-start(bf16[32,32,128]{2,1,0:T(8,128)(2,1)} %bitcast.18), calls=%async_computation.3 | async-start | bytes 524288 | tf_op jit(solution)/shard_map/all_to_all | solution.py:325
